TPU v7x, 256 devices: a whole 4x4x8 slice. The times are simulated.
256 devices in a mesh: sp: 32 (over z, y), tp: 8 (over x, core).
Axes of the slice: x: 4, y: 4, z: 8, core: 2. Of those that a mesh axis runs over, the one named last changes fastest.
Arguments:
- tokens: bfloat16 [24576, 4096], P('sp', 'tp'), may hold values from -6 to 6
- in_proj: bfloat16 [3, 4096, 1024], P(None, 'tp', 'sp'), may hold values from -0.09375 to 0.09375
- group_mix: bfloat16 [3, 4, 256, 256], replicated, may hold values from -0.375 to 0.375
- pool_gain: float32 [3, 1024], replicated, may hold values from 0.1 to 1.9
- out_proj: bfloat16 [3, 1024, 4096], P(None, 'sp', 'tp'), may hold values from -0.1875 to 0.1875
- norm_gain: float32 [3, 4096], P(None, 'tp'), may hold values from 0.25 to 3
- norm_bias: float32 [3, 4096], P(None, 'tp'), may hold values from -1.5 to 1.5
Outputs:
- stream_out: bfloat16 [24576, 4096], P('sp', 'tp')
All inputs are finite; a program needn't handle non-finite values.
Results may differ from a plain program's by a relative error of at most 0.017.
Values may be sent and summed in bfloat16 or wider, within the bound.
No kernel may reach another device: no remote copies, remote signals or barrier semaphores. Data moves between devices by JAX's collectives and lax.ppermute only.
A program may use at most 128 MiB of HBM per device.

v0:
```python
import functools

import jax
import jax.numpy as jnp
from jax import lax
from jax.experimental import pallas as pl
from jax.experimental.pallas import tpu as pltpu
from jax.sharding import Mesh
from jax.sharding import PartitionSpec as P


SP = ("z", "y")
norm_eps = 1e-05
REACH = 8
STAT = 16
F32, BF16 = jnp.float32, jnp.bfloat16
CORE_RUNS = (2, 2)
LIMITS = (60 * 2**20, 20 * 2**20)
VMEM_LIMIT = 20 * 2**20


def nbytes(shapes):
    return sum(s.size * s.dtype.itemsize for s in shapes)


def kernel_call(body, out_shape, scratch=(), flops=0, limit=VMEM_LIMIT, in_hbm=()):
    def call(*args):
        outs = out_shape if isinstance(out_shape, (list, tuple)) else [out_shape]
        specs = [pl.BlockSpec(memory_space=pltpu.SMEM)]
        specs += [
            pl.BlockSpec(memory_space=pl.ANY if i in in_hbm else pltpu.VMEM)
            for i in range(1, len(args))
        ]
        return pl.pallas_call(
            body,
            out_shape=out_shape,
            in_specs=specs,
            scratch_shapes=list(scratch),
            compiler_params=pltpu.CompilerParams(vmem_limit_bytes=limit),
            cost_estimate=pl.CostEstimate(
                flops=flops, bytes_accessed=nbytes(args) + nbytes(outs), transcendentals=0
            ),
        )(*args)

    return call


def dot(a, b):
    return lax.dot_general(a, b, (((1,), (0,)), ((), ())), preferred_element_type=F32)


def dot_t(a, b):
    return lax.dot_general(a, b, (((1,), (1,)), ((), ())), preferred_element_type=F32)


def parts(v):
    hi = v.astype(BF16).astype(F32)
    mid = (v - hi).astype(BF16).astype(F32)
    low = (v - hi - mid).astype(BF16).astype(F32)
    return hi, mid, low


def group_rows(weights, m, g, n):
    per = weights[0].shape[1] // n
    rows = [
        w[k, g * per + z, m] for z in range(per) for w in weights for k in range(w.shape[0])
    ]
    return jnp.concatenate(rows, axis=0)


def feature_rows(own, oth, m, g, n):
    return jnp.concatenate([group_rows(own, m, g, n), group_rows(oth, m, g, n)], axis=1)


def take(refs, *counts):
    out = []
    for m in counts:
        out.append(refs[:m])
        refs = refs[m:]
    return *out, refs


def project_body(sc, own, oth, *refs, n, held):
    w_own, w_oth, (*outs, held_out) = take(refs, *held)

    def project_group(k, carry):
        both = jnp.concatenate([own[...], oth[0 : own.shape[0], :]], axis=1)
        acc = dot_t(both, feature_rows(w_own, w_oth, 0, (sc[0] + k) % n, n))
        held_out[k] = acc.astype(BF16)
        return carry

    lax.fori_loop(0, n, project_group, 0)
    for k in range(n):
        outs[k][...] = held_out[k]


def pooled_mix(sc, proj, fetch, group_map, gains, out, layer, seq_length, ny, piece):
    rows_in, rows_out = proj.shape[0], out.shape[0]
    half = lax.shift_left(jnp.int32(1), sc[0])
    base = sc[1]
    col = lax.broadcasted_iota(jnp.int32, (rows_out, rows_in), 1) - REACH
    at = lax.broadcasted_iota(jnp.int32, (rows_out, 1), 0)
    low = jnp.maximum(at - half, -base)
    high = jnp.minimum(at + half, seq_length - base)
    band = jnp.where((col >= low) & (col < high), 1.0, 0.0).astype(BF16)
    count = jnp.maximum(high - low, 1).astype(F32)
    centre = proj.astype(F32)[REACH : REACH + rows_out]
    differ = (dot(band, proj) / count - centre).astype(BF16)
    width = proj.shape[1]
    true = lax.broadcasted_iota(jnp.int32, (width, width), 0)
    held = lax.broadcasted_iota(jnp.int32, (width, width), 1)
    z, k, i = held // (ny * piece), (held // piece) % ny, held % piece
    turn = jnp.where(true == (z * ny + (sc[2] + ny - k) % ny) * piece + i, 1.0, 0.0).astype(BF16)
    differ = dot_t(differ, turn).astype(BF16)
    gain = gains[layer : layer + 1, 0:width]
    for g in range(1, gains.shape[1] // width):
        gain = jnp.where(sc[0] == g, gains[layer : layer + 1, g * width : (g + 1) * width], gain)
    fetch.wait()
    mixed = (dot(differ, group_map[...]) * gain).astype(BF16)
    out[...] = dot(mixed, turn).astype(BF16)


def mix_first_body(sc, *refs, **sizes):
    *partials, maps, gains, out, group_map, sem = refs
    fetch = pltpu.make_async_copy(maps.at[sizes["layer"], sc[0]], group_map, sem)
    fetch.start()
    total = partials[0][...].astype(F32)
    for p in partials[1:]:
        total = total + p[...].astype(F32)
    pooled_mix(sc, total.astype(BF16), fetch, group_map, gains, out, **sizes)


def combine_stats(means, seconds, width):
    n = len(means)
    mean = means[0]
    for m in means[1:]:
        mean = mean + m
    mean = mean / n
    second = seconds[0] + width * jnp.square(means[0] - mean)
    for m, s in zip(means[1:], seconds[1:]):
        second = second + s + width * jnp.square(m - mean)
    return mean, lax.rsqrt(second / (n * width) + norm_eps)


def mix_body(sc, *refs, width, **sizes):
    *partials, maps, gains, out, row_out, group_map, sem = refs
    fetch = pltpu.make_async_copy(maps.at[sizes["layer"], sc[0]], group_map, sem)
    fetch.start()
    n = len(partials)
    rows = partials[0].shape[0] - 2 * STAT
    means, seconds, gw = [], [], []
    total, bw = None, None
    for p in partials:
        stat = jnp.concatenate(
            [p[rows : rows + STAT, :].astype(F32), p[rows + STAT :, :].astype(F32)], axis=1
        )
        means.append(stat[0:1] + stat[1:2] + stat[2:3])
        seconds.append(stat[3:4] + stat[4:5] + stat[5:6])
        chan = p[rows + STAT :, :].astype(F32)
        gw.append(chan[6:7] + chan[7:8] + chan[8:9])
        b = chan[9:10] + chan[10:11] + chan[11:12]
        bw = b if bw is None else bw + b
        q = p[0:rows, :].astype(F32)
        total = q if total is None else total + q
    mean, rstd = combine_stats(means, seconds, width)
    table = jnp.concatenate(
        [m - mean for m in means] + [mean, rstd, jnp.zeros((126 - n, mean.shape[1]), F32)], axis=0
    )
    table = jnp.transpose(table)[0:rows]
    row_out[...] = table
    for k in range(n):
        total = total + table[:, k : k + 1] * gw[k]
    proj = (total * table[:, n + 1 : n + 2] + bw).astype(BF16)
    pooled_mix(sc, proj, fetch, group_map, gains, out, **sizes)


def normed(resid, table, gain, bias, n):
    return (resid - table[:, n : n + 1]) * table[:, n + 1 : n + 2] * gain + bias


def branch_resid(sc, mixed, own, oth, w_own, w_oth, m, scale):
    n = len(mixed)
    block = jnp.concatenate([b[...] for b in mixed], axis=1)
    order = [(sc[0] + n - k) % n for k in range(n)]

    def branch(weights):
        return dot(block, jnp.concatenate([group_rows(weights, m, g, n) for g in order], axis=0))

    return scale * own + branch(w_own), scale * oth + branch(w_oth)


def centred(own, oth):
    width = own.shape[1] + oth.shape[1]
    mean = (jnp.sum(own, 1, keepdims=True) + jnp.sum(oth, 1, keepdims=True)) / width
    own, oth = own - mean, oth - mean
    second = jnp.sum(own * own, 1, keepdims=True) + jnp.sum(oth * oth, 1, keepdims=True)
    return own, oth, mean, second


def stat_rows(columns, rows, lanes):
    place = lax.broadcasted_iota(jnp.int32, (rows, 128), 1)
    table = jnp.zeros((rows, 128), F32)
    for i, c in enumerate(columns):
        table = jnp.where(place == i, c, table)
    if lanes > rows:
        table = jnp.concatenate([table, jnp.zeros((lanes - rows, 128), F32)], axis=0)
    return jnp.transpose(table)[0:STAT]


def norm_rows(norm, layer):
    layers = norm.shape[0] // 2
    return norm[layer : layer + 1, :], norm[layers + layer : layers + layer + 1, :]


def carried(slab, count):
    tail = slab[slab.shape[0] - 2 * STAT :, :].astype(F32)
    return tail[0:count] + tail[8 : 8 + count] + tail[16 : 16 + count]


def streams_in(refs, layer, rows, n):
    if layer == 0:
        own, oth, n_own, *rest = refs
        keep = slice(REACH, REACH + rows)
        n_oth = carried(oth, n_own.shape[0])
        return own[...].astype(F32)[keep], oth[...].astype(F32)[keep], [n_own, n_oth, *rest]
    own, oth, table, n_own, n_oth, *rest = refs
    keep = slice(REACH, REACH + rows)
    t = table[keep, :]
    s_own = normed(own[keep, :], t, *norm_rows(n_own, layer - 1), n).astype(BF16).astype(F32)
    n_oth = carried(n_oth, n_own.shape[0])
    s_oth = normed(oth[keep, :], t, *norm_rows(n_oth, layer - 1), n).astype(BF16).astype(F32)
    return s_own, s_oth, [n_own, n_oth, *rest]


def layer_body(sc, *refs, n, held, at, layer, scale):
    mixed, refs = refs[:n], refs[n:]
    rows = mixed[0].shape[0]
    own, oth, refs = streams_in(refs, layer, rows, n)
    (n_own, n_oth), w_own, w_oth, refs = take(refs, 2, *held)
    (g_own, b_own), (g_oth, b_oth) = norm_rows(n_own, layer), norm_rows(n_oth, layer)
    outs, (r_own, r_oth, lhs, held_out) = refs[:n], refs[n:]
    own, oth = branch_resid(sc, mixed, own, oth, w_own, w_oth, at, scale)
    r_own[...] = own
    r_oth[...] = oth
    own, oth, mean, second = centred(own, oth)
    width = outs[0].shape[1]
    stats = stat_rows(parts(mean) + parts(second), rows, 2 * width)
    feat = own.shape[1]
    for i, (value, gain, bias) in enumerate(((own, g_own, b_own), (oth, g_oth, b_oth))):
        cols = slice(i * feat, (i + 1) * feat)
        lhs[0:rows, cols] = (value * gain).astype(BF16)
        extra = parts(gain) + parts(bias)
        extra = jnp.concatenate(
            list(extra) + [jnp.zeros((STAT - 6, value.shape[1]), F32)], axis=0
        )
        lhs[rows : rows + STAT, cols] = extra.astype(BF16)
    place = lax.broadcasted_iota(jnp.int32, (STAT, width), 0)

    def project_group(k, carry):
        acc = dot_t(lhs[...], feature_rows(w_own, w_oth, at + 1, (sc[0] + k) % n, n))
        held_out[k, 0:rows, :] = acc[0:rows].astype(BF16)
        tail = acc[rows : rows + STAT]
        sums = parts(tail[0:1] + tail[1:2] + tail[2:3]) + parts(tail[3:4] + tail[4:5] + tail[5:6])
        block = stats[:, width:]
        for i, s in enumerate(sums):
            block = jnp.where(place == 6 + i, s, block)
        held_out[k, rows : rows + STAT, :] = stats[:, :width].astype(BF16)
        held_out[k, rows + STAT :, :] = block.astype(BF16)
        return carry

    lax.fori_loop(0, n, project_group, 0)
    for k in range(n):
        outs[k][...] = held_out[k]


def last_body(sc, *refs, n, held, at, layer, scale):
    mixed, refs = refs[:n], refs[n:]
    rows = mixed[0].shape[0]
    own, oth, refs = streams_in(refs, layer, rows, n)
    _, w_own, w_oth, (r_own, r_oth, stats) = take(refs, 2, *held)
    own, oth = branch_resid(sc, mixed, own, oth, w_own, w_oth, at, scale)
    r_own[...] = own
    r_oth[...] = oth
    _, _, mean, second = centred(own, oth)
    stats[...] = stat_rows((mean, second), rows, stats.shape[1])[0:8]


def finish_body(sc, *refs, width):
    stats, refs = refs[:2], refs[2:]
    r_own, r_oth, n_own, n_oth, out_own, out_oth = refs
    n_oth = carried(n_oth, n_own.shape[0])
    rows = r_own.shape[0]
    rows_of = [(s, i) for s in stats for i in range(0, s.shape[0], 8)]
    means = [s[i : i + 1, :] for s, i in rows_of]
    mean, rstd = combine_stats(means, [s[i + 1 : i + 2, :] for s, i in rows_of], width)
    table = jnp.concatenate([mean, rstd, jnp.zeros((126, mean.shape[1]), F32)], axis=0)
    table = jnp.transpose(table)[0:rows]
    at = pl.ds(pl.multiple_of(sc[3] * rows, 16), rows)
    out_own[at, :] = normed(r_own[...], table, *norm_rows(n_own, n_own.shape[0] // 2 - 1), 0).astype(BF16)
    out_oth[...] = normed(r_oth[...], table, *norm_rows(n_oth, n_oth.shape[0] // 2 - 1), 0).astype(BF16)


def shifted(array, axis, step):
    n = lax.axis_size(axis)
    return lax.ppermute(array, axis, [(i, (i + step) % n) for i in range(n)])


def other(array):
    return lax.ppermute(array, "c", [(0, 1), (1, 0)])


def after(value, *events):
    return lax.optimization_barrier((value, *events))[0]


def over_z(shards):
    spread = jnp.broadcast_to(shards[None], (lax.axis_size("z"), *shards.shape))
    return lax.all_to_all(spread, "z", 0, 0, tiled=True)


def over_y(block):
    return [block] + [shifted(block, "y", k) for k in range(1, lax.axis_size("y"))]


def over_c(own, sizes):
    runs = []
    for size in sizes:
        runs.append(jnp.stack(own[:size]) if size > 1 else own[0][None])
        own = own[size:]
    return runs, [other(b) for b in runs]


def layers_on_device(tokens, in_proj, group_mix, pool_gain, out_proj, norm_gain, norm_bias):
    rows_dev, feat = tokens.shape
    layers = in_proj.shape[0]
    n = lax.axis_size("x")
    sp = lax.axis_size(SP)
    seq_length = rows_dev * sp
    channels = in_proj.shape[2] * sp
    group = channels // n
    half_rows = rows_dev // 2
    pad = layers * REACH
    scale = (2.0 * layers) ** 0.25
    x, c = lax.axis_index("x"), lax.axis_index("c")
    start = lax.axis_index(SP) * rows_dev + c * half_rows

    def scalars(base):
        return jnp.stack([x, base, lax.axis_index("y"), c]).astype(jnp.int32)

    sc = scalars(start)
    ny = lax.axis_size("y")
    sizes = dict(seq_length=seq_length, ny=ny, piece=in_proj.shape[2])
    in_t = jnp.swapaxes(in_proj, 1, 2)
    z_in = over_z(in_t[:1])
    w_in = over_c(over_y(z_in), CORE_RUNS)

    up = [(i, i + 1) for i in range(sp - 1)]
    before = lax.ppermute(tokens[rows_dev - pad :], SP, up)
    behind = lax.ppermute(tokens[:pad], SP, [(j, i) for i, j in up])
    wide = jnp.concatenate([before, tokens, behind], axis=0)
    length = half_rows + 2 * pad
    mine = lax.dynamic_slice_in_dim(wide, c * half_rows, length, 0)
    theirs = lax.dynamic_slice_in_dim(wide, (1 - c) * half_rows, length, 0)
    norm = jnp.concatenate([norm_gain, norm_bias], axis=0)
    rest, tail = norm, []
    for _ in range(3):
        part = lax.reduce_precision(rest, 8, 7)
        tail.append(jnp.pad(part.astype(BF16), ((0, 8 - norm.shape[0]), (0, 0))))
        rest = rest - part
    tail.append(jnp.zeros_like(tail[0]))
    theirs = other(jnp.concatenate([theirs, *tail], axis=0))
    norms = (norm, theirs)

    def block(rows, width, dtype=BF16):
        return jax.ShapeDtypeStruct((rows, width), dtype)

    def exchanged(blocks):
        return [blocks[0]] + [shifted(b, "x", k) for k, b in enumerate(blocks) if k]

    rows = length
    flops = 2 * rows * 2 * feat * channels
    partials = kernel_call(
        functools.partial(project_body, n=n, held=(len(w_in[0]), len(w_in[1]))),
        [block(rows, group)] * n,
        flops=flops,
        scratch=[pltpu.VMEM((n, rows, group), BF16)],
    )(sc, mine, theirs, *w_in[0], *w_in[1])
    stream = [mine, theirs]
    late = [w for l in range(1, layers) for w in (out_proj[l], in_t[min(l + 1, layers - 1)])]
    z_a = over_z(jnp.stack([out_proj[0], in_t[1]]))
    for l in range(layers):
        first, last = l == 0, l == layers - 1
        arrived = exchanged(partials)
        if first:
            y_w = over_y(after(z_a, partials[0]))
        done = rows - 2 * REACH
        here = scalars(start - pad + (l + 1) * REACH)
        mix_flops = 2 * done * group * (rows + group)
        if first:
            mixed = kernel_call(
                functools.partial(mix_first_body, layer=l, **sizes),
                block(done, group),
                flops=mix_flops,
                scratch=[pltpu.VMEM((group, group), BF16), pltpu.SemaphoreType.DMA(())],
                in_hbm=(n + 1,),
            )(here, *arrived, group_mix, pool_gain)
        else:
            mixed, table = kernel_call(
                functools.partial(mix_body, width=2 * feat, layer=l, **sizes),
                [block(done, group), block(rows, 128, F32)],
                flops=mix_flops,
                scratch=[pltpu.VMEM((group, group), BF16), pltpu.SemaphoreType.DMA(())],
                in_hbm=(n + 1,),
            )(here, *arrived, group_mix, pool_gain)
            stream = stream + [table]
        all_mixed = exchanged([mixed] * n)
        if first:
            z_b = over_z(after(jnp.stack(late[:-1]), z_a, partials[0]))
            y_w = lax.optimization_barrier((*y_w, mixed))[:-1]
            own_w, oth_w = over_c(list(y_w), CORE_RUNS)
            y_w = over_y(z_b)
        elif l == 1:
            y_w = lax.optimization_barrier((*y_w, mixed))[:-1]
            own_w, oth_w = over_c(list(y_w), CORE_RUNS)
        held = (len(own_w), len(oth_w))
        at = 2 * max(l - 1, 0)
        rows = done
        resid = [block(rows, feat, F32)] * 2
        if not last:
            *partials, r_own, r_oth = kernel_call(
                functools.partial(layer_body, n=n, held=held, at=at, layer=l, scale=scale),
                [block(rows + 2 * STAT, group)] * n + resid,
                scratch=[
                    pltpu.VMEM((rows + STAT, 2 * feat), BF16),
                    pltpu.VMEM((n, rows + 2 * STAT, group), BF16),
                ],
                flops=4 * rows * 2 * feat * channels,
                limit=LIMITS[l],
            )(here, *all_mixed, *stream, *(norms[:1] if first else norms), *own_w, *oth_w)
            stream = [r_own, r_oth]
        else:
            r_own, r_oth, stats = kernel_call(
                functools.partial(last_body, n=n, held=held, at=at, layer=l, scale=scale),
                resid + [block(8, rows, F32)],
                flops=2 * rows * 2 * feat * channels,
            )(here, *all_mixed, *stream, *(norms[:1] if first else norms), *own_w, *oth_w)
            near = lax.ppermute(stats, "x", [(i, i ^ 1) for i in range(n)])
            stats = jnp.concatenate([stats, near], axis=0)
            far = lax.ppermute(stats, "x", [(i, i ^ 2) for i in range(n)])
            out_own, out_oth = kernel_call(
                functools.partial(finish_body, width=2 * feat),
                [block(rows_dev, feat), block(rows, feat)],
            )(here, stats, far, r_own, r_oth, *norms)
    return lax.dynamic_update_slice_in_dim(out_own, other(out_oth), (1 - c) * half_rows, 0)


def solution(mesh):
    split = Mesh(mesh.devices.reshape(8, 4, 4, 2), ("z", "y", "x", "c"))
    tp = ("x", "c")
    in_specs = (P(SP, tp), P(None, tp, SP), P(), P(), P(None, SP, tp), P(None, tp), P(None, tp))
    return jax.shard_map(
        layers_on_device, mesh=split, in_specs=in_specs, out_specs=P(SP, tp), check_vma=False
    )
```

profile of v0, /device:TPU:128, one launch (start us, length us, event | category | flops | bytes accessed | tf_op | source)
XLA Modules:
  0.0 208.7 jit_solution(8690599648215799538)
XLA Ops:
  0.8 4.5 %collective-permute-start.1 = (bf16[24,512]{1,0:T(8,128)(2,1)S(1)}, bf16[24,512]{1,0:T(8,128)(2,1)S(1)}, u32[]{:S(2)}, u32[]{:S(2)}) collective-permute-start(bf16[24,512]{1,0:T(8,128)(2,1)S(1)} %get-tuple-element.77), channel_id=1, source_target_pairs={{8,0},{16,8},{24,16},{32,24},{40,32},{48,40},{56,48},{64,56},{72,6... | collective-permute-start | bytes 73736 | tf_op jit(solution)/shard_map/ppermute | solution.py:359
  9.4 7.7 %all-to-all-start = ((bf16[8,1,32,512]{3,2,1,0:T(8,128)(2,1)}), bf16[8,1,32,512]{3,2,1,0:T(8,128)(2,1)S(1)}, u32[]{:S(2)}, u32[]{:S(2)}) async-start(bf16[8,1,32,512]{3,2,1,0:T(8,128)(2,1)} %broadcast_in_dim.12), calls=%async_computation | async-start | bytes 524288 | tf_op jit(solution)/shard_map/all_to_all | solution.py:318
  19.4 3.9 %all-to-all-done = bf16[8,1,32,512]{3,2,1,0:T(8,128)(2,1)S(1)} async-done(((bf16[8,1,32,512]{3,2,1,0:T(8,128)(2,1)}), bf16[8,1,32,512]{3,2,1,0:T(8,128)(2,1)S(1)}, u32[]{:S(2)}, u32[]{:S(2)}) %all-to-all-start) | async-done | bytes 262176 | tf_op jit(solution)/shard_map/all_to_all | solution.py:318
  24.1 9.4 %all-to-all-start.1 = ((bf16[8,2,32,512]{3,2,1,0:T(8,128)(2,1)}), bf16[8,2,32,512]{3,2,1,0:T(8,128)(2,1)}, u32[]{:S(2)}, u32[]{:S(2)}) async-start(bf16[8,2,32,512]{3,2,1,0:T(8,128)(2,1)} %broadcast_in_dim.26), calls=%async_computation.1 | async-start | bytes 1048576 | tf_op jit(solution)/shard_map/all_to_all | solution.py:318
  34.5 3.6 %collective-permute-start.5 = (bf16[8,1,32,512]{3,2,0,1:T(8,128)(2,1)S(1)}, bf16[8,1,32,512]{3,2,0,1:T(8,128)(2,1)S(1)}, u32[]{:S(2)}, u32[]{:S(2)}) collective-permute-start(bf16[8,1,32,512]{3,2,0,1:T(8,128)(2,1)S(1)} %bitcast.23), channel_id=1, source_target_pairs={{0,24},{8,0},{16,8},{24,16},{1,25},{9,1},{17,9},{25,17},{2,26},{10... | collective-permute-start | bytes 786440 | tf_op jit(solution)/shard_map/ppermute | solution.py:305
  40.7 3.6 %collective-permute-done.3 = bf16[8,1,32,512]{3,2,0,1:T(8,128)(2,1)S(1)} collective-permute-done((bf16[8,1,32,512]{3,2,0,1:T(8,128)(2,1)S(1)}, bf16[8,1,32,512]{3,2,0,1:T(8,128)(2,1)S(1)}, u32[]{:S(2)}, u32[]{:S(2)}) %collective-permute-start.3) | collective-permute-done | bytes 262176 | tf_op jit(solution)/shard_map/ppermute | solution.py:305
  44.4 2.5 %collective-permute-done.5 = bf16[8,1,32,512]{3,2,0,1:T(8,128)(2,1)S(1)} collective-permute-done((bf16[8,1,32,512]{3,2,0,1:T(8,128)(2,1)S(1)}, bf16[8,1,32,512]{3,2,0,1:T(8,128)(2,1)S(1)}, u32[]{:S(2)}, u32[]{:S(2)}) %collective-permute-start.5) | collective-permute-done | bytes 262176 | tf_op jit(solution)/shard_map/ppermute | solution.py:305
  51.2 3.0 %shard_map.73 = (bf16[432,256]{1,0:T(8,128)(2,1)S(1)}, bf16[432,256]{1,0:T(8,128)(2,1)}, bf16[432,256]{1,0:T(8,128)(2,1)S(1)}, bf16[432,256]{1,0:T(8,128)(2,1)S(1)}) custom-call(s32[4]{0:T(128)S(1)} %add_add_fusion.sc, bf16[432,512]{1,0:T(8,128)(2,1)S(1)} %get-tuple-element.76.own.refs_4_, bf16[464,512]{1,0:T(8,128)(2,1)S(1)} %collective-permute-done.2.oth.refs_5_.refs_8_, ...), custom_call_target="tpu_custom_call" | custom-call | flops 905969664 | bytes 3899408 | tf_op jit(solution)/shard_map/pallas_call | solution.py:34
  56.4 2.4 %collective-permute-start.16 = (bf16[8,2,32,512]{3,2,1,0:T(8,128)(2,1)}, bf16[8,2,32,512]{3,2,1,0:T(8,128)(2,1)}, u32[]{:S(2)}, u32[]{:S(2)}) collective-permute-start(bf16[8,2,32,512]{3,2,1,0:T(8,128)(2,1)} %all-to-all-done.1), channel_id=1, source_target_pairs={{0,24},{8,0},{16,8},{24,16},{1,25},{9,1},{17,9},{25,17},{2,26},{10... | collective-permute-start | bytes 1572872 | tf_op jit(solution)/shard_map/ppermute | solution.py:305
  60.2 2.7 %collective-permute-start.9 = (bf16[432,256]{1,0:T(8,128)(2,1)}, bf16[432,256]{1,0:T(8,128)(2,1)S(1)}, u32[]{:S(2)}, u32[]{:S(2)}) collective-permute-start(bf16[432,256]{1,0:T(8,128)(2,1)} %copy-done.11), channel_id=1, source_target_pairs={{0,4},{2,6},{4,0},{6,2},{1,5},{3,7},{5,1},{7,3},{8,12},{10,14},{12... | collective-permute-start | bytes 663560 | tf_op jit(solution)/shard_map/ppermute | solution.py:305
  64.0 2.1 %collective-permute-start.10 = (bf16[432,256]{1,0:T(8,128)(2,1)S(1)}, bf16[432,256]{1,0:T(8,128)(2,1)S(1)}, u32[]{:S(2)}, u32[]{:S(2)}) collective-permute-start(bf16[432,256]{1,0:T(8,128)(2,1)S(1)} %get-tuple-element.43), channel_id=1, source_target_pairs={{0,6},{2,0},{4,2},{6,4},{1,7},{3,1},{5,3},{7,5},{8,14},{10,8},{12,... | collective-permute-start | bytes 663560 | tf_op jit(solution)/shard_map/ppermute | solution.py:305
  67.9 7.2 %all-to-all-start.2 = ((bf16[8,3,32,512]{3,2,1,0:T(8,128)(2,1)}), bf16[8,3,32,512]{3,2,1,0:T(8,128)(2,1)}, u32[]{:S(2)}, u32[]{:S(2)}) async-start(bf16[8,3,32,512]{3,2,1,0:T(8,128)(2,1)} %broadcast_in_dim.27), calls=%async_computation.2 | async-start | bytes 1572864 | tf_op jit(solution)/shard_map/all_to_all | solution.py:318
  76.9 4.8 %collective-permute-done.16 = bf16[8,2,32,512]{3,2,1,0:T(8,128)(2,1)} collective-permute-done((bf16[8,2,32,512]{3,2,1,0:T(8,128)(2,1)}, bf16[8,2,32,512]{3,2,1,0:T(8,128)(2,1)}, u32[]{:S(2)}, u32[]{:S(2)}) %collective-permute-start.16) | collective-permute-done | bytes 524320 | tf_op jit(solution)/shard_map/ppermute | solution.py:305
  81.8 3.7 %collective-permute-done.14 = bf16[8,2,32,512]{3,2,1,0:T(8,128)(2,1)} collective-permute-done((bf16[8,2,32,512]{3,2,1,0:T(8,128)(2,1)}, bf16[8,2,32,512]{3,2,1,0:T(8,128)(2,1)}, u32[]{:S(2)}, u32[]{:S(2)}) %collective-permute-start.14) | collective-permute-done | bytes 524320 | tf_op jit(solution)/shard_map/ppermute | solution.py:305
  85.5 2.3 %pad_maximum_fusion.3.refs_8_ = bf16[2,8,2,32,512]{4,3,2,1,0:T(8,128)(2,1)} fusion(bf16[1,8,2,32,512]{4,3,2,1,0:T(8,128)(2,1)} %bitcast.16, bf16[1,8,2,32,512]{4,3,2,1,0:T(8,128)(2,1)} %bitcast.15), kind=kLoop, calls=%fused_computation.3 | loop fusion | flops 524288 | bytes 2097152 | tf_op jit(solution)/shard_map/stack | solution.py:328
  93.8 7.1 %collective-permute-done.13.refs_3_ = bf16[416,256]{1,0:T(8,128)(2,1)S(1)} collective-permute-done((bf16[416,256]{1,0:T(8,128)(2,1)S(1)}, bf16[416,256]{1,0:T(8,128)(2,1)S(1)}, u32[]{:S(2)}, u32[]{:S(2)}) %collective-permute-start.13) | collective-permute-done | bytes 213024 | tf_op jit(solution)/shard_map/ppermute | solution.py:305
  102.5 2.1 %collective-permute-done.11.refs_1_ = bf16[416,256]{1,0:T(8,128)(2,1)S(1)} collective-permute-done((bf16[416,256]{1,0:T(8,128)(2,1)S(1)}, bf16[416,256]{1,0:T(8,128)(2,1)S(1)}, u32[]{:S(2)}, u32[]{:S(2)}) %collective-permute-start.11) | collective-permute-done | bytes 213024 | tf_op jit(solution)/shard_map/ppermute | solution.py:305
  105.4 7.4 %shard_map.75 = (bf16[448,256]{1,0:T(8,128)(2,1)}, bf16[448,256]{1,0:T(8,128)(2,1)}, bf16[448,256]{1,0:T(8,128)(2,1)}, bf16[448,256]{1,0:T(8,128)(2,1)}, f32[416,512]{1,0:T(8,128)}, /*index=5*/f32[416,512]{1,0:T(8,128)}) custom-call(s32[4]{0:T(128)} %copy-done.10, bf16[416,256]{1,0:T(8,128)(2,1)} %copy-done.8, bf16[416,256]{1,0:T(8,128)(2,1)} %copy-done.16, ...), custom_call_target="tpu_custom_call" | custom-call | flops 1744830464 | bytes 8597520 | tf_op jit(solution)/shard_map/pallas_call | solution.py:34
  113.4 3.1 %collective-permute-start.20 = (bf16[448,256]{1,0:T(8,128)(2,1)}, bf16[448,256]{1,0:T(8,128)(2,1)S(1)}, u32[]{:S(2)}, u32[]{:S(2)}) collective-permute-start(bf16[448,256]{1,0:T(8,128)(2,1)} %get-tuple-element.51), channel_id=1, source_target_pairs={{0,4},{2,6},{4,0},{6,2},{1,5},{3,7},{5,1},{7,3},{8,12},{10,14},{12... | collective-permute-start | bytes 688136 | tf_op jit(solution)/shard_map/ppermute | solution.py:305
  116.5 10.2 %collective-permute-done.19.refs_1_ = bf16[448,256]{1,0:T(8,128)(2,1)S(1)} collective-permute-done((bf16[448,256]{1,0:T(8,128)(2,1)}, bf16[448,256]{1,0:T(8,128)(2,1)S(1)}, u32[]{:S(2)}, u32[]{:S(2)}) %collective-permute-start.19) | collective-permute-done | bytes 229408 | tf_op jit(solution)/shard_map/ppermute | solution.py:305
  126.8 6.9 %collective-permute-done.21.refs_3_ = bf16[448,256]{1,0:T(8,128)(2,1)S(1)} collective-permute-done((bf16[448,256]{1,0:T(8,128)(2,1)}, bf16[448,256]{1,0:T(8,128)(2,1)S(1)}, u32[]{:S(2)}, u32[]{:S(2)}) %collective-permute-start.21) | collective-permute-done | bytes 229408 | tf_op jit(solution)/shard_map/ppermute | solution.py:305
  134.6 2.1 %shard_map.76 = (bf16[400,256]{1,0:T(8,128)(2,1)S(1)}, f32[416,128]{1,0:T(8,128)S(1)}) custom-call(s32[4]{0:T(128)S(1)} %add_add_fusion.1.sc, bf16[448,256]{1,0:T(8,128)(2,1)S(1)} %copy-done.7, bf16[448,256]{1,0:T(8,128)(2,1)S(1)} %collective-permute-done.19.refs_1_, bf16[448,256]{1,0:T(8,128)(2,1)S(1)} %collective-permute-done.20.refs_2_, ...), custom_call_target="tpu_custom_call" | custom-call | flops 137625600 | bytes 2920464 | tf_op jit(solution)/shard_map/pallas_call | solution.py:34
  141.3 4.5 %collective-permute-start.24 = (bf16[400,256]{1,0:T(8,128)(2,1)S(1)}, bf16[400,256]{1,0:T(8,128)(2,1)S(1)}, u32[]{:S(2)}, u32[]{:S(2)}) collective-permute-start(bf16[400,256]{1,0:T(8,128)(2,1)S(1)} %get-tuple-element.53.refs_0_), channel_id=1, source_target_pairs={{0,6},{2,0},{4,2},{6,4},{1,7},{3,1},{5,3},{7,5},{8,14},{10,8},{12,... | collective-permute-start | bytes 614408 | tf_op jit(solution)/shard_map/ppermute | solution.py:305
  147.3 7.5 %collective-permute-done.24.refs_3_ = bf16[400,256]{1,0:T(8,128)(2,1)S(1)} collective-permute-done((bf16[400,256]{1,0:T(8,128)(2,1)S(1)}, bf16[400,256]{1,0:T(8,128)(2,1)S(1)}, u32[]{:S(2)}, u32[]{:S(2)}) %collective-permute-start.24) | collective-permute-done | bytes 204832 | tf_op jit(solution)/shard_map/ppermute | solution.py:305
  155.3 3.2 %collective-permute-done.22.refs_1_ = bf16[400,256]{1,0:T(8,128)(2,1)S(1)} collective-permute-done((bf16[400,256]{1,0:T(8,128)(2,1)S(1)}, bf16[400,256]{1,0:T(8,128)(2,1)S(1)}, u32[]{:S(2)}, u32[]{:S(2)}) %collective-permute-start.22) | collective-permute-done | bytes 204832 | tf_op jit(solution)/shard_map/ppermute | solution.py:305
  158.6 4.0 %shard_map.77 = (bf16[432,256]{1,0:T(8,128)(2,1)S(1)}, bf16[432,256]{1,0:T(8,128)(2,1)S(1)}, bf16[432,256]{1,0:T(8,128)(2,1)S(1)}, bf16[432,256]{1,0:T(8,128)(2,...) custom-call(s32[4]{0:T(128)S(1)} %add_add_fusion.1.sc, bf16[400,256]{1,0:T(8,128)(2,1)S(1)} %get-tuple-element.53.refs_0_, ...), custom_call_target="tpu_custom_call" | custom-call | flops 1677721600 | bytes 12038160 | tf_op jit(solution)/shard_map/pallas_call | solution.py:34
  166.7 9.2 %collective-permute-done.30.refs_1_ = bf16[432,256]{1,0:T(8,128)(2,1)S(1)} collective-permute-done((bf16[432,256]{1,0:T(8,128)(2,1)S(1)}, bf16[432,256]{1,0:T(8,128)(2,1)S(1)}, u32[]{:S(2)}, u32[]{:S(2)}) %collective-permute-start.30) | collective-permute-done | bytes 221216 | tf_op jit(solution)/shard_map/ppermute | solution.py:305
  178.6 2.7 %collective-permute-start.35 = (bf16[384,256]{1,0:T(8,128)(2,1)S(1)}, bf16[384,256]{1,0:T(8,128)(2,1)S(1)}, u32[]{:S(2)}, u32[]{:S(2)}) collective-permute-start(bf16[384,256]{1,0:T(8,128)(2,1)S(1)} %get-tuple-element.66.refs_0_), channel_id=1, source_target_pairs={{0,6},{2,0},{4,2},{6,4},{1,7},{3,1},{5,3},{7,5},{8,14},{10,8},{12,... | collective-permute-start | bytes 589832 | tf_op jit(solution)/shard_map/ppermute | solution.py:305
  182.3 7.6 %collective-permute-done.35.refs_3_ = bf16[384,256]{1,0:T(8,128)(2,1)S(1)} collective-permute-done((bf16[384,256]{1,0:T(8,128)(2,1)S(1)}, bf16[384,256]{1,0:T(8,128)(2,1)S(1)}, u32[]{:S(2)}, u32[]{:S(2)}) %collective-permute-start.35) | collective-permute-done | bytes 196640 | tf_op jit(solution)/shard_map/ppermute | solution.py:305
  190.6 2.7 %collective-permute-done.33.refs_1_ = bf16[384,256]{1,0:T(8,128)(2,1)S(1)} collective-permute-done((bf16[384,256]{1,0:T(8,128)(2,1)S(1)}, bf16[384,256]{1,0:T(8,128)(2,1)S(1)}, u32[]{:S(2)}, u32[]{:S(2)}) %collective-permute-start.33) | collective-permute-done | bytes 196640 | tf_op jit(solution)/shard_map/ppermute | solution.py:305
  195.2 3.7 %collective-permute-done.36 = f32[8,384]{1,0:T(8,128)S(1)} collective-permute-done((f32[8,384]{1,0:T(8,128)S(1)}, f32[8,384]{1,0:T(8,128)S(1)}, u32[]{:S(2)}, u32[]{:S(2)}) %collective-permute-start.36) | collective-permute-done | bytes 12320 | tf_op jit(solution)/shard_map/ppermute | solution.py:447
  199.5 4.8 %collective-permute-done.37.refs_1_ = f32[16,384]{1,0:T(8,128)S(1)} collective-permute-done((f32[16,384]{1,0:T(8,128)S(1)}, f32[16,384]{1,0:T(8,128)S(1)}, u32[]{:S(2)}, u32[]{:S(2)}) %collective-permute-start.37) | collective-permute-done | bytes 24608 | tf_op jit(solution)/shard_map/ppermute | solution.py:449
  (122 shorter events, 56.1 us)
Async XLA Ops:
  0.8 17.6 %collective-permute-start.1 = (bf16[24,512]{1,0:T(8,128)(2,1)S(1)}, bf16[24,512]{1,0:T(8,128)(2,1)S(1)}, u32[]{:S(2)}, u32[]{:S(2)}) collective-permute-start(bf16[24,512]{1,0:T(8,128)(2,1)S(1)} %get-tuple-element.77), channel_id=1, source_target_pairs={{8,0},{16,8},{24,16},{32,24},{40,32},{48,40},{56,48},{64,56},{72,6... | collective-permute-start | bytes 73736 | tf_op jit(solution)/shard_map/ppermute | solution.py:359
  5.3 13.1 %collective-permute-start = (bf16[24,512]{1,0:T(8,128)(2,1)S(1)}, bf16[24,512]{1,0:T(8,128)(2,1)S(1)}, u32[]{:S(2)}, u32[]{:S(2)}) collective-permute-start(bf16[24,512]{1,0:T(8,128)(2,1)S(1)} %get-tuple-element.78), channel_id=1, source_target_pairs={{0,8},{8,16},{16,24},{24,32},{32,40},{40,48},{48,56},{56,64},{64,7... | collective-permute-start | bytes 73736 | tf_op jit(solution)/shard_map/ppermute | solution.py:358
  9.4 13.9 %all-to-all-start = ((bf16[8,1,32,512]{3,2,1,0:T(8,128)(2,1)}), bf16[8,1,32,512]{3,2,1,0:T(8,128)(2,1)S(1)}, u32[]{:S(2)}, u32[]{:S(2)}) async-start(bf16[8,1,32,512]{3,2,1,0:T(8,128)(2,1)} %broadcast_in_dim.12), calls=%async_computation | async-start | bytes 524288 | tf_op jit(solution)/shard_map/all_to_all | solution.py:318
  24.1 32.2 %all-to-all-start.1 = ((bf16[8,2,32,512]{3,2,1,0:T(8,128)(2,1)}), bf16[8,2,32,512]{3,2,1,0:T(8,128)(2,1)}, u32[]{:S(2)}, u32[]{:S(2)}) async-start(bf16[8,2,32,512]{3,2,1,0:T(8,128)(2,1)} %broadcast_in_dim.26), calls=%async_computation.1 | async-start | bytes 1048576 | tf_op jit(solution)/shard_map/all_to_all | solution.py:318
  33.6 10.7 %collective-permute-start.3 = (bf16[8,1,32,512]{3,2,0,1:T(8,128)(2,1)S(1)}, bf16[8,1,32,512]{3,2,0,1:T(8,128)(2,1)S(1)}, u32[]{:S(2)}, u32[]{:S(2)}) collective-permute-start(bf16[8,1,32,512]{3,2,0,1:T(8,128)(2,1)S(1)} %bitcast.22), channel_id=1, source_target_pairs={{0,8},{8,16},{16,24},{24,0},{1,9},{9,17},{17,25},{25,1},{2,10},{10... | collective-permute-start | bytes 786440 | tf_op jit(solution)/shard_map/ppermute | solution.py:305
  34.5 12.5 %collective-permute-start.5 = (bf16[8,1,32,512]{3,2,0,1:T(8,128)(2,1)S(1)}, bf16[8,1,32,512]{3,2,0,1:T(8,128)(2,1)S(1)}, u32[]{:S(2)}, u32[]{:S(2)}) collective-permute-start(bf16[8,1,32,512]{3,2,0,1:T(8,128)(2,1)S(1)} %bitcast.23), channel_id=1, source_target_pairs={{0,24},{8,0},{16,8},{24,16},{1,25},{9,1},{17,9},{25,17},{2,26},{10... | collective-permute-start | bytes 786440 | tf_op jit(solution)/shard_map/ppermute | solution.py:305
  38.0 10.2 %collective-permute-start.4 = (bf16[8,1,32,512]{3,2,0,1:T(8,128)(2,1)S(1)}, bf16[8,1,32,512]{3,2,0,1:T(8,128)(2,1)S(1)}, u32[]{:S(2)}, u32[]{:S(2)}) collective-permute-start(bf16[8,1,32,512]{3,2,0,1:T(8,128)(2,1)S(1)} %bitcast.24), channel_id=1, source_target_pairs={{0,16},{8,24},{16,0},{24,8},{1,17},{9,25},{17,1},{25,9},{2,18},{10... | collective-permute-start | bytes 786440 | tf_op jit(solution)/shard_map/ppermute | solution.py:305
  56.4 25.4 %collective-permute-start.16 = (bf16[8,2,32,512]{3,2,1,0:T(8,128)(2,1)}, bf16[8,2,32,512]{3,2,1,0:T(8,128)(2,1)}, u32[]{:S(2)}, u32[]{:S(2)}) collective-permute-start(bf16[8,2,32,512]{3,2,1,0:T(8,128)(2,1)} %all-to-all-done.1), channel_id=1, source_target_pairs={{0,24},{8,0},{16,8},{24,16},{1,25},{9,1},{17,9},{25,17},{2,26},{10... | collective-permute-start | bytes 1572872 | tf_op jit(solution)/shard_map/ppermute | solution.py:305
  58.8 23.0 %collective-permute-start.15 = (bf16[8,2,32,512]{3,2,1,0:T(8,128)(2,1)}, bf16[8,2,32,512]{3,2,1,0:T(8,128)(2,1)}, u32[]{:S(2)}, u32[]{:S(2)}) collective-permute-start(bf16[8,2,32,512]{3,2,1,0:T(8,128)(2,1)} %all-to-all-done.1), channel_id=1, source_target_pairs={{0,16},{8,24},{16,0},{24,8},{1,17},{9,25},{17,1},{25,9},{2,18},{10... | collective-permute-start | bytes 1572872 | tf_op jit(solution)/shard_map/ppermute | solution.py:305
  60.2 25.3 %collective-permute-start.14 = (bf16[8,2,32,512]{3,2,1,0:T(8,128)(2,1)}, bf16[8,2,32,512]{3,2,1,0:T(8,128)(2,1)}, u32[]{:S(2)}, u32[]{:S(2)}) collective-permute-start(bf16[8,2,32,512]{3,2,1,0:T(8,128)(2,1)} %all-to-all-done.1), channel_id=1, source_target_pairs={{0,8},{8,16},{16,24},{24,0},{1,9},{9,17},{17,25},{25,1},{2,10},{10... | collective-permute-start | bytes 1572872 | tf_op jit(solution)/shard_map/ppermute | solution.py:305
  60.2 15.0 %collective-permute-start.9 = (bf16[432,256]{1,0:T(8,128)(2,1)}, bf16[432,256]{1,0:T(8,128)(2,1)S(1)}, u32[]{:S(2)}, u32[]{:S(2)}) collective-permute-start(bf16[432,256]{1,0:T(8,128)(2,1)} %copy-done.11), channel_id=1, source_target_pairs={{0,4},{2,6},{4,0},{6,2},{1,5},{3,7},{5,1},{7,3},{8,12},{10,14},{12... | collective-permute-start | bytes 663560 | tf_op jit(solution)/shard_map/ppermute | solution.py:305
  64.0 11.2 %collective-permute-start.10 = (bf16[432,256]{1,0:T(8,128)(2,1)S(1)}, bf16[432,256]{1,0:T(8,128)(2,1)S(1)}, u32[]{:S(2)}, u32[]{:S(2)}) collective-permute-start(bf16[432,256]{1,0:T(8,128)(2,1)S(1)} %get-tuple-element.43), channel_id=1, source_target_pairs={{0,6},{2,0},{4,2},{6,4},{1,7},{3,1},{5,3},{7,5},{8,14},{10,8},{12,... | collective-permute-start | bytes 663560 | tf_op jit(solution)/shard_map/ppermute | solution.py:305
  67.9 33.1 %all-to-all-start.2 = ((bf16[8,3,32,512]{3,2,1,0:T(8,128)(2,1)}), bf16[8,3,32,512]{3,2,1,0:T(8,128)(2,1)}, u32[]{:S(2)}, u32[]{:S(2)}) async-start(bf16[8,3,32,512]{3,2,1,0:T(8,128)(2,1)} %broadcast_in_dim.27), calls=%async_computation.2 | async-start | bytes 1572864 | tf_op jit(solution)/shard_map/all_to_all | solution.py:318
  87.8 16.9 %collective-permute-start.18 = (bf16[2,8,2,32,512]{4,3,2,1,0:T(8,128)(2,1)}, bf16[2,8,2,32,512]{4,3,2,1,0:T(8,128)(2,1)}, u32[]{:S(2)}, u32[]{:S(2)}) collective-permute-start(bf16[2,8,2,32,512]{4,3,2,1,0:T(8,128)(2,1)} %pad_maximum_fusion.3.refs_8_), channel_id=1, source_target_pairs={{0,1},{1,0},{2,3},{3,2},{4,5},{5,4},{6,7},{7,6},{8,9},{9,8},{10,11... | collective-permute-start | bytes 3145736 | tf_op jit(solution)/shard_map/ppermute | solution.py:309
  89.1 15.6 %collective-permute-start.17 = (bf16[2,8,2,32,512]{4,3,2,1,0:T(8,128)(2,1)S(1)}, bf16[2,8,2,32,512]{4,3,2,1,0:T(8,128)(2,1)}, u32[]{:S(2)}, u32[]{:S(2)}) collective-permute-start(bf16[2,8,2,32,512]{4,3,2,1,0:T(8,128)(2,1)S(1)} %pad_maximum_fusion.2.refs_7_), channel_id=1, source_target_pairs={{0,1},{1,0},{2,3},{3,2},{4,5},{5,4},{6,7},{7,6},{8,9},{9,8},{10,11... | collective-permute-start | bytes 3145736 | tf_op jit(solution)/shard_map/ppermute | solution.py:309
  89.7 11.3 %collective-permute-start.13 = (bf16[416,256]{1,0:T(8,128)(2,1)S(1)}, bf16[416,256]{1,0:T(8,128)(2,1)S(1)}, u32[]{:S(2)}, u32[]{:S(2)}) collective-permute-start(bf16[416,256]{1,0:T(8,128)(2,1)S(1)} %shard_map.74.refs_0_), channel_id=1, source_target_pairs={{0,6},{2,0},{4,2},{6,4},{1,7},{3,1},{5,3},{7,5},{8,14},{10,8},{12,... | collective-permute-start | bytes 638984 | tf_op jit(solution)/shard_map/ppermute | solution.py:305
  91.4 10.2 %collective-permute-start.12 = (bf16[416,256]{1,0:T(8,128)(2,1)S(1)}, bf16[416,256]{1,0:T(8,128)(2,1)S(1)}, u32[]{:S(2)}, u32[]{:S(2)}) collective-permute-start(bf16[416,256]{1,0:T(8,128)(2,1)S(1)} %shard_map.74.refs_0_), channel_id=1, source_target_pairs={{0,4},{2,6},{4,0},{6,2},{1,5},{3,7},{5,1},{7,3},{8,12},{10,14},{12... | collective-permute-start | bytes 638984 | tf_op jit(solution)/shard_map/ppermute | solution.py:305
  93.3 11.4 %collective-permute-start.11 = (bf16[416,256]{1,0:T(8,128)(2,1)S(1)}, bf16[416,256]{1,0:T(8,128)(2,1)S(1)}, u32[]{:S(2)}, u32[]{:S(2)}) collective-permute-start(bf16[416,256]{1,0:T(8,128)(2,1)S(1)} %shard_map.74.refs_0_), channel_id=1, source_target_pairs={{0,2},{2,4},{4,6},{6,0},{1,3},{3,5},{5,7},{7,1},{8,10},{10,12},{12... | collective-permute-start | bytes 638984 | tf_op jit(solution)/shard_map/ppermute | solution.py:305
  101.0 35.8 %collective-permute-start.27 = (bf16[8,3,32,512]{3,2,1,0:T(8,128)(2,1)}, bf16[8,3,32,512]{3,2,1,0:T(8,128)(2,1)}, u32[]{:S(2)}, u32[]{:S(2)}) collective-permute-start(bf16[8,3,32,512]{3,2,1,0:T(8,128)(2,1)} %all-to-all-done.2), channel_id=1, source_target_pairs={{0,24},{8,0},{16,8},{24,16},{1,25},{9,1},{17,9},{25,17},{2,26},{10... | collective-permute-start | bytes 2359304 | tf_op jit(solution)/shard_map/ppermute | solution.py:305
  101.6 35.2 %collective-permute-start.26 = (bf16[8,3,32,512]{3,2,1,0:T(8,128)(2,1)}, bf16[8,3,32,512]{3,2,1,0:T(8,128)(2,1)}, u32[]{:S(2)}, u32[]{:S(2)}) collective-permute-start(bf16[8,3,32,512]{3,2,1,0:T(8,128)(2,1)} %all-to-all-done.2), channel_id=1, source_target_pairs={{0,16},{8,24},{16,0},{24,8},{1,17},{9,25},{17,1},{25,9},{2,18},{10... | collective-permute-start | bytes 2359304 | tf_op jit(solution)/shard_map/ppermute | solution.py:305
  104.7 32.7 %collective-permute-start.25 = (bf16[8,3,32,512]{3,2,1,0:T(8,128)(2,1)}, bf16[8,3,32,512]{3,2,1,0:T(8,128)(2,1)}, u32[]{:S(2)}, u32[]{:S(2)}) collective-permute-start(bf16[8,3,32,512]{3,2,1,0:T(8,128)(2,1)} %all-to-all-done.2), channel_id=1, source_target_pairs={{0,8},{8,16},{16,24},{24,0},{1,9},{9,17},{17,25},{25,1},{2,10},{10... | collective-permute-start | bytes 2359304 | tf_op jit(solution)/shard_map/ppermute | solution.py:305
  112.8 13.9 %collective-permute-start.19 = (bf16[448,256]{1,0:T(8,128)(2,1)}, bf16[448,256]{1,0:T(8,128)(2,1)S(1)}, u32[]{:S(2)}, u32[]{:S(2)}) collective-permute-start(bf16[448,256]{1,0:T(8,128)(2,1)} %get-tuple-element.50), channel_id=1, source_target_pairs={{0,2},{2,4},{4,6},{6,0},{1,3},{3,5},{5,7},{7,1},{8,10},{10,12},{12... | collective-permute-start | bytes 688136 | tf_op jit(solution)/shard_map/ppermute | solution.py:305
  113.4 13.4 %collective-permute-start.20 = (bf16[448,256]{1,0:T(8,128)(2,1)}, bf16[448,256]{1,0:T(8,128)(2,1)S(1)}, u32[]{:S(2)}, u32[]{:S(2)}) collective-permute-start(bf16[448,256]{1,0:T(8,128)(2,1)} %get-tuple-element.51), channel_id=1, source_target_pairs={{0,4},{2,6},{4,0},{6,2},{1,5},{3,7},{5,1},{7,3},{8,12},{10,14},{12... | collective-permute-start | bytes 688136 | tf_op jit(solution)/shard_map/ppermute | solution.py:305
  138.9 19.6 %collective-permute-start.29 = (bf16[2,8,3,32,512]{4,3,2,1,0:T(8,128)(2,1)S(1)}, bf16[2,8,3,32,512]{4,3,2,1,0:T(8,128)(2,1)S(1)}, u32[]{:S(2)}, u32[]{:S(2)}) collective-permute-start(bf16[2,8,3,32,512]{4,3,2,1,0:T(8,128)(2,1)S(1)} %pad_maximum_fusion.1.refs_10_), channel_id=1, source_target_pairs={{0,1},{1,0},{2,3},{3,2},{4,5},{5,4},{6,7},{7,6},{8,9},{9,8},{10,11... | collective-permute-start | bytes 4718600 | tf_op jit(solution)/shard_map/ppermute | solution.py:309
  140.7 17.8 %collective-permute-start.28 = (bf16[2,8,3,32,512]{4,3,2,1,0:T(8,128)(2,1)S(1)}, bf16[2,8,3,32,512]{4,3,2,1,0:T(8,128)(2,1)S(1)}, u32[]{:S(2)}, u32[]{:S(2)}) collective-permute-start(bf16[2,8,3,32,512]{4,3,2,1,0:T(8,128)(2,1)S(1)} %pad_maximum_fusion.refs_9_), channel_id=1, source_target_pairs={{0,1},{1,0},{2,3},{3,2},{4,5},{5,4},{6,7},{7,6},{8,9},{9,8},{10,11... | collective-permute-start | bytes 4718600 | tf_op jit(solution)/shard_map/ppermute | solution.py:309
  141.3 13.6 %collective-permute-start.24 = (bf16[400,256]{1,0:T(8,128)(2,1)S(1)}, bf16[400,256]{1,0:T(8,128)(2,1)S(1)}, u32[]{:S(2)}, u32[]{:S(2)}) collective-permute-start(bf16[400,256]{1,0:T(8,128)(2,1)S(1)} %get-tuple-element.53.refs_0_), channel_id=1, source_target_pairs={{0,6},{2,0},{4,2},{6,4},{1,7},{3,1},{5,3},{7,5},{8,14},{10,8},{12,... | collective-permute-start | bytes 614408 | tf_op jit(solution)/shard_map/ppermute | solution.py:305
  147.3 11.2 %collective-permute-start.22 = (bf16[400,256]{1,0:T(8,128)(2,1)S(1)}, bf16[400,256]{1,0:T(8,128)(2,1)S(1)}, u32[]{:S(2)}, u32[]{:S(2)}) collective-permute-start(bf16[400,256]{1,0:T(8,128)(2,1)S(1)} %get-tuple-element.53.refs_0_), channel_id=1, source_target_pairs={{0,2},{2,4},{4,6},{6,0},{1,3},{3,5},{5,7},{7,1},{8,10},{10,12},{12... | collective-permute-start | bytes 614408 | tf_op jit(solution)/shard_map/ppermute | solution.py:305
  162.5 13.4 %collective-permute-start.30 = (bf16[432,256]{1,0:T(8,128)(2,1)S(1)}, bf16[432,256]{1,0:T(8,128)(2,1)S(1)}, u32[]{:S(2)}, u32[]{:S(2)}) collective-permute-start(bf16[432,256]{1,0:T(8,128)(2,1)S(1)} %get-tuple-element.63), channel_id=1, source_target_pairs={{0,2},{2,4},{4,6},{6,0},{1,3},{3,5},{5,7},{7,1},{8,10},{10,12},{12... | collective-permute-start | bytes 663560 | tf_op jit(solution)/shard_map/ppermute | solution.py:305
  162.6 13.3 %collective-permute-start.31 = (bf16[432,256]{1,0:T(8,128)(2,1)S(1)}, bf16[432,256]{1,0:T(8,128)(2,1)S(1)}, u32[]{:S(2)}, u32[]{:S(2)}) collective-permute-start(bf16[432,256]{1,0:T(8,128)(2,1)S(1)} %get-tuple-element.64), channel_id=1, source_target_pairs={{0,4},{2,6},{4,0},{6,2},{1,5},{3,7},{5,1},{7,3},{8,12},{10,14},{12... | collective-permute-start | bytes 663560 | tf_op jit(solution)/shard_map/ppermute | solution.py:305
  164.7 11.9 %collective-permute-start.32 = (bf16[432,256]{1,0:T(8,128)(2,1)S(1)}, bf16[432,256]{1,0:T(8,128)(2,1)S(1)}, u32[]{:S(2)}, u32[]{:S(2)}) collective-permute-start(bf16[432,256]{1,0:T(8,128)(2,1)S(1)} %get-tuple-element.65), channel_id=1, source_target_pairs={{0,6},{2,0},{4,2},{6,4},{1,7},{3,1},{5,3},{7,5},{8,14},{10,8},{12,... | collective-permute-start | bytes 663560 | tf_op jit(solution)/shard_map/ppermute | solution.py:305
  178.6 11.3 %collective-permute-start.35 = (bf16[384,256]{1,0:T(8,128)(2,1)S(1)}, bf16[384,256]{1,0:T(8,128)(2,1)S(1)}, u32[]{:S(2)}, u32[]{:S(2)}) collective-permute-start(bf16[384,256]{1,0:T(8,128)(2,1)S(1)} %get-tuple-element.66.refs_0_), channel_id=1, source_target_pairs={{0,6},{2,0},{4,2},{6,4},{1,7},{3,1},{5,3},{7,5},{8,14},{10,8},{12,... | collective-permute-start | bytes 589832 | tf_op jit(solution)/shard_map/ppermute | solution.py:305
  181.6 11.7 %collective-permute-start.33 = (bf16[384,256]{1,0:T(8,128)(2,1)S(1)}, bf16[384,256]{1,0:T(8,128)(2,1)S(1)}, u32[]{:S(2)}, u32[]{:S(2)}) collective-permute-start(bf16[384,256]{1,0:T(8,128)(2,1)S(1)} %get-tuple-element.66.refs_0_), channel_id=1, source_target_pairs={{0,2},{2,4},{4,6},{6,0},{1,3},{3,5},{5,7},{7,1},{8,10},{10,12},{12... | collective-permute-start | bytes 589832 | tf_op jit(solution)/shard_map/ppermute | solution.py:305
  (27 other events, 283.2 us)
where the time goes:
time: 212 us; the launch traced here: 209 us
  waiting for transfers between devices  91.8 us (43%)
  starting transfers between devices  72 us (34%)
  Pallas kernels  24.1 us (11%)
  local copies, waits for them, and re-layouts  11.2 us (5%)
  other arithmetic  9.23 us (4%)
    ppermute x27, waiting for transfers between devices, shifted(): return lax.ppermute(array, axis, [(i, (i + step) % n) for i in range(n)])  76.1 us
    ppermute x27, starting transfers between devices, shifted(): return lax.ppermute(array, axis, [(i, (i + step) % n) for i in range(n)])  38.7 us
    all_to_all x3, starting transfers between devices, over_z(): return lax.all_to_all(spread, 'z', 0, 0, tiled=True)  24.3 us
    pallas_call x8, Pallas kernels, call(): pl.pallas_call(body, out_shape=out_shape, in_specs=specs, scratch_shapes=...  24.1 us
    another operation x6, other arithmetic, over_c(): runs.append(jnp.stack(own[:size]) if size > 1 else own[0][None])  6.9 us
    unnamed x41, local copies, waits for them, and re-layouts  5.03 us
    ppermute x1, waiting for transfers between devices, layers_on_device(): far = lax.ppermute(stats, 'x', [(i, i ^ 2) for i in range(n)])  4.76 us
    ppermute x1, starting transfers between devices, layers_on_device(): behind = lax.ppermute(tokens[:pad], SP, [(j, i) for i, j in up])  4.46 us
  transfers between devices with their start and end apart: 42, of which 24 were waited for; matrix products, arithmetic and copies ran while one was open for 7% of the time, Pallas kernels for 7%

commit v1 on v0

--- a/solution.py
+++ b/solution.py
@@ -80,18 +80,30 @@
     return *out, refs
 
 
+def spread(held, outs):
+    rows = held.shape[1]
+    size = max(m for m in range(16, 97, 16) if rows % m == 0)
+
+    def copy(i, carry):
+        at = pl.ds(pl.multiple_of(i * size, 16), size)
+        for k, out in enumerate(outs):
+            out[at, :] = held[k, at, :]
+        return carry
+
+    lax.fori_loop(0, rows // size, copy, 0)
+
+
 def project_body(sc, own, oth, *refs, n, held):
     w_own, w_oth, (*outs, held_out) = take(refs, *held)
 
     def project_group(k, carry):
-        both = jnp.concatenate([own[...], oth[0 : own.shape[0], :]], axis=1)
+        both = jnp.concatenate([own[...], oth[...]], axis=1)
         acc = dot_t(both, feature_rows(w_own, w_oth, 0, (sc[0] + k) % n, n))
         held_out[k] = acc.astype(BF16)
         return carry
 
     lax.fori_loop(0, n, project_group, 0)
-    for k in range(n):
-        outs[k][...] = held_out[k]
+    spread(held_out, outs)
 
 
 def pooled_mix(sc, proj, fetch, group_map, gains, out, layer, seq_length, ny, piece):
@@ -212,22 +224,15 @@
     return norm[layer : layer + 1, :], norm[layers + layer : layers + layer + 1, :]
 
 
-def carried(slab, count):
-    tail = slab[slab.shape[0] - 2 * STAT :, :].astype(F32)
-    return tail[0:count] + tail[8 : 8 + count] + tail[16 : 16 + count]
-
-
 def streams_in(refs, layer, rows, n):
     if layer == 0:
-        own, oth, n_own, *rest = refs
+        own, oth, *rest = refs
         keep = slice(REACH, REACH + rows)
-        n_oth = carried(oth, n_own.shape[0])
-        return own[...].astype(F32)[keep], oth[...].astype(F32)[keep], [n_own, n_oth, *rest]
+        return own[...].astype(F32)[keep], oth[...].astype(F32)[keep], rest
     own, oth, table, n_own, n_oth, *rest = refs
     keep = slice(REACH, REACH + rows)
     t = table[keep, :]
     s_own = normed(own[keep, :], t, *norm_rows(n_own, layer - 1), n).astype(BF16).astype(F32)
-    n_oth = carried(n_oth, n_own.shape[0])
     s_oth = normed(oth[keep, :], t, *norm_rows(n_oth, layer - 1), n).astype(BF16).astype(F32)
     return s_own, s_oth, [n_own, n_oth, *rest]
 
@@ -269,8 +274,7 @@
         return carry
 
     lax.fori_loop(0, n, project_group, 0)
-    for k in range(n):
-        outs[k][...] = held_out[k]
+    spread(held_out, outs)
 
 
 def last_body(sc, *refs, n, held, at, layer, scale):
@@ -285,14 +289,11 @@
     stats[...] = stat_rows((mean, second), rows, stats.shape[1])[0:8]
 
 
-def finish_body(sc, *refs, width):
-    stats, refs = refs[:2], refs[2:]
+def finish_body(sc, *refs, n, width):
+    stats, refs = refs[:n], refs[n:]
     r_own, r_oth, n_own, n_oth, out_own, out_oth = refs
-    n_oth = carried(n_oth, n_own.shape[0])
     rows = r_own.shape[0]
-    rows_of = [(s, i) for s in stats for i in range(0, s.shape[0], 8)]
-    means = [s[i : i + 1, :] for s, i in rows_of]
-    mean, rstd = combine_stats(means, [s[i + 1 : i + 2, :] for s, i in rows_of], width)
+    mean, rstd = combine_stats([s[0:1, :] for s in stats], [s[1:2, :] for s in stats], width)
     table = jnp.concatenate([mean, rstd, jnp.zeros((126, mean.shape[1]), F32)], axis=0)
     table = jnp.transpose(table)[0:rows]
     at = pl.ds(pl.multiple_of(sc[3] * rows, 16), rows)
@@ -322,12 +323,17 @@
     return [block] + [shifted(block, "y", k) for k in range(1, lax.axis_size("y"))]
 
 
-def over_c(own, sizes):
-    runs = []
+def over_c(own, sizes, event=None):
+    runs, swapped = [], []
     for size in sizes:
-        runs.append(jnp.stack(own[:size]) if size > 1 else own[0][None])
+        now = own[:size]
+        if event is not None:
+            now = lax.optimization_barrier((*now, event))[:-1]
+        event = jnp.stack(now) if size > 1 else now[0][None]
+        runs.append(event)
+        swapped.append(other(event))
         own = own[size:]
-    return runs, [other(b) for b in runs]
+    return runs, swapped
 
 
 def layers_on_device(tokens, in_proj, group_mix, pool_gain, out_proj, norm_gain, norm_bias):
@@ -350,8 +356,9 @@
     sc = scalars(start)
     ny = lax.axis_size("y")
     sizes = dict(seq_length=seq_length, ny=ny, piece=in_proj.shape[2])
-    in_t = jnp.swapaxes(in_proj, 1, 2)
-    z_in = over_z(in_t[:1])
+    first_in = jnp.swapaxes(in_proj[:1], 1, 2)
+    in_t = [None, *jnp.swapaxes(after(in_proj[1:], first_in), 1, 2)]
+    z_in = over_z(first_in)
     w_in = over_c(over_y(z_in), CORE_RUNS)
 
     up = [(i, i + 1) for i in range(sp - 1)]
@@ -360,16 +367,10 @@
     wide = jnp.concatenate([before, tokens, behind], axis=0)
     length = half_rows + 2 * pad
     mine = lax.dynamic_slice_in_dim(wide, c * half_rows, length, 0)
-    theirs = lax.dynamic_slice_in_dim(wide, (1 - c) * half_rows, length, 0)
+    theirs = other(lax.dynamic_slice_in_dim(wide, (1 - c) * half_rows, length, 0))
     norm = jnp.concatenate([norm_gain, norm_bias], axis=0)
-    rest, tail = norm, []
-    for _ in range(3):
-        part = lax.reduce_precision(rest, 8, 7)
-        tail.append(jnp.pad(part.astype(BF16), ((0, 8 - norm.shape[0]), (0, 0))))
-        rest = rest - part
-    tail.append(jnp.zeros_like(tail[0]))
-    theirs = other(jnp.concatenate([theirs, *tail], axis=0))
-    norms = (norm, theirs)
+    norms = (norm, other(norm))
+    mine = after(mine, norms[1])
 
     def block(rows, width, dtype=BF16):
         return jax.ShapeDtypeStruct((rows, width), dtype)
@@ -415,13 +416,11 @@
             stream = stream + [table]
         all_mixed = exchanged([mixed] * n)
         if first:
-            z_b = over_z(after(jnp.stack(late[:-1]), z_a, partials[0]))
-            y_w = lax.optimization_barrier((*y_w, mixed))[:-1]
-            own_w, oth_w = over_c(list(y_w), CORE_RUNS)
+            z_b = over_z(jnp.stack(late[:-1]))
+            own_w, oth_w = over_c(y_w, CORE_RUNS, mixed)
             y_w = over_y(z_b)
         elif l == 1:
-            y_w = lax.optimization_barrier((*y_w, mixed))[:-1]
-            own_w, oth_w = over_c(list(y_w), CORE_RUNS)
+            own_w, oth_w = over_c(y_w, (ny,), mixed)
         held = (len(own_w), len(oth_w))
         at = 2 * max(l - 1, 0)
         rows = done
@@ -436,21 +435,18 @@
                 ],
                 flops=4 * rows * 2 * feat * channels,
                 limit=LIMITS[l],
-            )(here, *all_mixed, *stream, *(norms[:1] if first else norms), *own_w, *oth_w)
+            )(here, *all_mixed, *stream, *norms, *own_w, *oth_w)
             stream = [r_own, r_oth]
         else:
             r_own, r_oth, stats = kernel_call(
                 functools.partial(last_body, n=n, held=held, at=at, layer=l, scale=scale),
                 resid + [block(8, rows, F32)],
                 flops=2 * rows * 2 * feat * channels,
-            )(here, *all_mixed, *stream, *(norms[:1] if first else norms), *own_w, *oth_w)
-            near = lax.ppermute(stats, "x", [(i, i ^ 1) for i in range(n)])
-            stats = jnp.concatenate([stats, near], axis=0)
-            far = lax.ppermute(stats, "x", [(i, i ^ 2) for i in range(n)])
+            )(here, *all_mixed, *stream, *norms, *own_w, *oth_w)
             out_own, out_oth = kernel_call(
-                functools.partial(finish_body, width=2 * feat),
+                functools.partial(finish_body, n=n, width=2 * feat),
                 [block(rows_dev, feat), block(rows, feat)],
-            )(here, stats, far, r_own, r_oth, *norms)
+            )(here, *exchanged([stats] * n), r_own, r_oth, *norms)
     return lax.dynamic_update_slice_in_dim(out_own, other(out_oth), (1 - c) * half_rows, 0)
 
 

time: 212 us -> 200 us (0.943)
  waiting for transfers between devices: 91.8 us -> 81.2 us
  other arithmetic: 9.23 us -> 6.95 us
    ppermute x2 -> x0, waiting for transfers between devices: 8.43 us -> none  [the longest x1 4.76 us: layers_on_device(): far = lax.ppermute(stats, 'x', [(i, i ^ 2) for i in range(n)])]
    all_to_all x3, waiting for transfers between devices: 3.95 us -> 0.04 us  [over_z(): return lax.all_to_all(spread, 'z', 0, 0, tiled=True)]
    all_to_all x3, starting transfers between devices: 24.3 us -> 21.8 us  [over_z(): return lax.all_to_all(spread, 'z', 0, 0, tiled=True)]
    unnamed x41 -> x42, local copies, waits for them, and re-layouts: 5.03 us -> 3.03 us
    ppermute x27 -> x30, waiting for transfers between devices: 76.1 us -> 77.9 us  [shifted(): return lax.ppermute(array, axis, [(i, (i + step) % n) for i in range(n)])]
    another operation x7 -> x6, other arithmetic: 7.67 us -> 6.71 us  [the longest x5 6.69 us: over_c(): event = jnp.stack(now) if size > 1 else now[0][None]]
    ppermute x27 -> x30, starting transfers between devices: 38.7 us -> 39.6 us  [shifted(): return lax.ppermute(array, axis, [(i, (i + step) % n) for i in range(n)])]
  transfers between devices with their start and end apart: 42 -> 43, of which waited for: 24 -> 21; matrix products, arithmetic and copies ran while one was open for 7% -> 5% of each run, Pallas kernels for 7% -> 8%
where the time goes in v1:
time: 200 us; the launch traced here: 196 us
  waiting for transfers between devices  81.2 us (41%)
  starting transfers between devices  71.9 us (36%)
  Pallas kernels  25.4 us (13%)
  local copies, waits for them, and re-layouts  10.4 us (5%)
  other arithmetic  6.95 us (3%)
    ppermute x30, waiting for transfers between devices, shifted(): return lax.ppermute(array, axis, [(i, (i + step) % n) for i in range(n)])  77.9 us
    ppermute x30, starting transfers between devices, shifted(): return lax.ppermute(array, axis, [(i, (i + step) % n) for i in range(n)])  39.6 us
    pallas_call x8, Pallas kernels, call(): pl.pallas_call(body, out_shape=out_shape, in_specs=specs, scratch_shapes=...  25.4 us
    all_to_all x3, starting transfers between devices, over_z(): return lax.all_to_all(spread, 'z', 0, 0, tiled=True)  21.8 us
    another operation x5, other arithmetic, over_c(): event = jnp.stack(now) if size > 1 else now[0][None]  6.69 us
    ppermute x1, starting transfers between devices, layers_on_device(): behind = lax.ppermute(tokens[:pad], SP, [(j, i) for i, j in up])  5.68 us
  transfers between devices with their start and end apart: 43, of which 21 were waited for; matrix products, arithmetic and copies ran while one was open for 5% of the time, Pallas kernels for 8%

profile of v1, /device:TPU:128, one launch (start us, length us, event | category | flops | bytes accessed | tf_op | source)
XLA Modules:
  0.0 196.2 jit_solution(46066775992666168)
XLA Ops:
  1.6 7.2 %all-to-all-start = ((bf16[8,1,32,512]{3,2,1,0:T(8,128)(2,1)}), bf16[8,1,32,512]{3,2,1,0:T(8,128)(2,1)S(1)}, u32[]{:S(2)}, u32[]{:S(2)}) async-start(bf16[8,1,32,512]{3,2,1,0:T(8,128)(2,1)} %broadcast_in_dim.9), calls=%async_computation | async-start | bytes 524288 | tf_op jit(solution)/shard_map/all_to_all | solution.py:319
  9.5 3.5 %collective-permute-start = (bf16[24,512]{1,0:T(8,128)(2,1)S(1)}, bf16[24,512]{1,0:T(8,128)(2,1)S(1)}, u32[]{:S(2)}, u32[]{:S(2)}) collective-permute-start(bf16[24,512]{1,0:T(8,128)(2,1)S(1)} %get-tuple-element.84), channel_id=1, source_target_pairs={{0,8},{8,16},{16,24},{24,32},{32,40},{40,48},{48,56},{56,64},{64,7... | collective-permute-start | bytes 73736 | tf_op jit(solution)/shard_map/ppermute | solution.py:365
  13.0 5.7 %collective-permute-start.1 = (bf16[24,512]{1,0:T(8,128)(2,1)S(1)}, bf16[24,512]{1,0:T(8,128)(2,1)S(1)}, u32[]{:S(2)}, u32[]{:S(2)}) collective-permute-start(bf16[24,512]{1,0:T(8,128)(2,1)S(1)} %get-tuple-element.83), channel_id=1, source_target_pairs={{8,0},{16,8},{24,16},{32,24},{40,32},{48,40},{56,48},{64,56},{72,6... | collective-permute-start | bytes 73736 | tf_op jit(solution)/shard_map/ppermute | solution.py:366
  21.2 7.3 %all-to-all-start.1 = ((bf16[8,2,32,512]{3,2,1,0:T(8,128)(2,1)}), bf16[8,2,32,512]{3,2,1,0:T(8,128)(2,1)}, u32[]{:S(2)}, u32[]{:S(2)}) async-start(bf16[8,2,32,512]{3,2,1,0:T(8,128)(2,1)} %broadcast_in_dim.10), calls=%async_computation.1 | async-start | bytes 1048576 | tf_op jit(solution)/shard_map/all_to_all | solution.py:319
  32.0 9.8 %collective-permute-done.4 = bf16[8,1,32,512]{3,2,0,1:T(8,128)(2,1)S(1)} collective-permute-done((bf16[8,1,32,512]{3,2,0,1:T(8,128)(2,1)S(1)}, bf16[8,1,32,512]{3,2,0,1:T(8,128)(2,1)S(1)}, u32[]{:S(2)}, u32[]{:S(2)}) %collective-permute-start.4) | collective-permute-done | bytes 262176 | tf_op jit(solution)/shard_map/ppermute | solution.py:306
  45.7 3.9 %shard_map.73 = (bf16[432,256]{1,0:T(8,128)(2,1)S(1)}, bf16[432,256]{1,0:T(8,128)(2,1)S(1)}, bf16[432,256]{1,0:T(8,128)(2,1)}, bf16[432,256]{1,0:T(8,128)(2,1)S(1)}) custom-call(s32[4]{0:T(128)S(1)} %add_add_fusion.sc, bf16[432,512]{1,0:T(8,128)(2,1)S(1)} %get-tuple-element.43.own.refs_4_, bf16[432,512]{1,0:T(8,128)(2,1)} %collective-permute-done.3.oth.refs_5_, ...), custom_call_target="tpu_custom_call" | custom-call | flops 905969664 | bytes 3866640 | tf_op jit(solution)/shard_map/pallas_call | solution.py:34
  50.9 3.0 %collective-permute-start.10 = (bf16[432,256]{1,0:T(8,128)(2,1)}, bf16[432,256]{1,0:T(8,128)(2,1)S(1)}, u32[]{:S(2)}, u32[]{:S(2)}) collective-permute-start(bf16[432,256]{1,0:T(8,128)(2,1)} %get-tuple-element.48), channel_id=1, source_target_pairs={{0,4},{2,6},{4,0},{6,2},{1,5},{3,7},{5,1},{7,3},{8,12},{10,14},{12... | collective-permute-start | bytes 663560 | tf_op jit(solution)/shard_map/ppermute | solution.py:306
  54.2 3.6 %collective-permute-start.16 = (bf16[8,2,32,512]{3,2,1,0:T(8,128)(2,1)}, bf16[8,2,32,512]{3,2,1,0:T(8,128)(2,1)}, u32[]{:S(2)}, u32[]{:S(2)}) collective-permute-start(bf16[8,2,32,512]{3,2,1,0:T(8,128)(2,1)} %all-to-all-done.1), channel_id=1, source_target_pairs={{0,16},{8,24},{16,0},{24,8},{1,17},{9,25},{17,1},{25,9},{2,18},{10... | collective-permute-start | bytes 1572872 | tf_op jit(solution)/shard_map/ppermute | solution.py:306
  63.4 7.2 %all-to-all-start.2 = ((bf16[8,3,32,512]{3,2,1,0:T(8,128)(2,1)}), bf16[8,3,32,512]{3,2,1,0:T(8,128)(2,1)}, u32[]{:S(2)}, u32[]{:S(2)}) async-start(bf16[8,3,32,512]{3,2,1,0:T(8,128)(2,1)} %broadcast_in_dim.11), calls=%async_computation.2 | async-start | bytes 1572864 | tf_op jit(solution)/shard_map/all_to_all | solution.py:319
  72.5 2.4 %pad_maximum_fusion.1.refs_8_ = bf16[2,8,2,32,512]{4,3,2,1,0:T(8,128)(2,1)} fusion(bf16[1,8,2,32,512]{4,3,2,1,0:T(8,128)(2,1)} %bitcast.15, bf16[1,8,2,32,512]{4,3,2,1,0:T(8,128)(2,1)} %bitcast.14), kind=kLoop, calls=%fused_computation.1 | loop fusion | flops 524288 | bytes 2097152 | tf_op jit(solution)/shard_map/stack | solution.py:332
  74.9 6.4 %collective-permute-done.16 = bf16[8,2,32,512]{3,2,1,0:T(8,128)(2,1)} collective-permute-done((bf16[8,2,32,512]{3,2,1,0:T(8,128)(2,1)}, bf16[8,2,32,512]{3,2,1,0:T(8,128)(2,1)}, u32[]{:S(2)}, u32[]{:S(2)}) %collective-permute-start.16) | collective-permute-done | bytes 524320 | tf_op jit(solution)/shard_map/ppermute | solution.py:306
  81.3 2.3 %pad_maximum_fusion.2.refs_9_ = bf16[2,8,2,32,512]{4,3,2,1,0:T(8,128)(2,1)} fusion(bf16[1,8,2,32,512]{4,3,2,1,0:T(8,128)(2,1)} %bitcast.17, bf16[1,8,2,32,512]{4,3,2,1,0:T(8,128)(2,1)} %bitcast.16), kind=kLoop, calls=%fused_computation.2 | loop fusion | flops 524288 | bytes 2097152 | tf_op jit(solution)/shard_map/stack | solution.py:332
  87.4 9.6 %collective-permute-done.12.refs_1_ = bf16[416,256]{1,0:T(8,128)(2,1)S(1)} collective-permute-done((bf16[416,256]{1,0:T(8,128)(2,1)S(1)}, bf16[416,256]{1,0:T(8,128)(2,1)S(1)}, u32[]{:S(2)}, u32[]{:S(2)}) %collective-permute-start.12) | collective-permute-done | bytes 213024 | tf_op jit(solution)/shard_map/ppermute | solution.py:306
  97.3 3.8 %collective-permute-start.27 = (bf16[8,3,32,512]{3,2,1,0:T(8,128)(2,1)}, bf16[8,3,32,512]{3,2,1,0:T(8,128)(2,1)}, u32[]{:S(2)}, u32[]{:S(2)}) collective-permute-start(bf16[8,3,32,512]{3,2,1,0:T(8,128)(2,1)} %all-to-all-done.2), channel_id=1, source_target_pairs={{0,16},{8,24},{16,0},{24,8},{1,17},{9,25},{17,1},{25,9},{2,18},{10... | collective-permute-start | bytes 2359304 | tf_op jit(solution)/shard_map/ppermute | solution.py:306
  101.8 7.7 %shard_map.75 = (bf16[448,256]{1,0:T(8,128)(2,1)}, bf16[448,256]{1,0:T(8,128)(2,1)}, bf16[448,256]{1,0:T(8,128)(2,1)}, bf16[448,256]{1,0:T(8,128)(2,1)}, f32[416,512]{1,0:T(8,128)}, /*index=5*/f32[416,512]{1,0:T(8,128)}) custom-call(s32[4]{0:T(128)} %copy-done.11, bf16[416,256]{1,0:T(8,128)(2,1)} %copy-done.7, bf16[416,256]{1,0:T(8,128)(2,1)} %copy-done.17, ...), custom_call_target="tpu_custom_call" | custom-call | flops 1744830464 | bytes 8577040 | tf_op jit(solution)/shard_map/pallas_call | solution.py:34
  109.5 2.4 %collective-permute-start.21 = (bf16[448,256]{1,0:T(8,128)(2,1)}, bf16[448,256]{1,0:T(8,128)(2,1)S(1)}, u32[]{:S(2)}, u32[]{:S(2)}) collective-permute-start(bf16[448,256]{1,0:T(8,128)(2,1)} %get-tuple-element.58), channel_id=1, source_target_pairs={{0,4},{2,6},{4,0},{6,2},{1,5},{3,7},{5,1},{7,3},{8,12},{10,14},{12... | collective-permute-start | bytes 688136 | tf_op jit(solution)/shard_map/ppermute | solution.py:306
  111.8 6.5 %collective-permute-done.20.refs_1_ = bf16[448,256]{1,0:T(8,128)(2,1)S(1)} collective-permute-done((bf16[448,256]{1,0:T(8,128)(2,1)}, bf16[448,256]{1,0:T(8,128)(2,1)S(1)}, u32[]{:S(2)}, u32[]{:S(2)}) %collective-permute-start.20) | collective-permute-done | bytes 229408 | tf_op jit(solution)/shard_map/ppermute | solution.py:306
  119.1 2.8 %collective-permute-done.21.refs_2_ = bf16[448,256]{1,0:T(8,128)(2,1)S(1)} collective-permute-done((bf16[448,256]{1,0:T(8,128)(2,1)}, bf16[448,256]{1,0:T(8,128)(2,1)S(1)}, u32[]{:S(2)}, u32[]{:S(2)}) %collective-permute-start.21) | collective-permute-done | bytes 229408 | tf_op jit(solution)/shard_map/ppermute | solution.py:306
  121.9 2.7 %collective-permute-done.22.refs_3_ = bf16[448,256]{1,0:T(8,128)(2,1)S(1)} collective-permute-done((bf16[448,256]{1,0:T(8,128)(2,1)}, bf16[448,256]{1,0:T(8,128)(2,1)S(1)}, u32[]{:S(2)}, u32[]{:S(2)}) %collective-permute-start.22) | collective-permute-done | bytes 229408 | tf_op jit(solution)/shard_map/ppermute | solution.py:306
  125.5 2.1 %shard_map.76 = (bf16[400,256]{1,0:T(8,128)(2,1)S(1)}, f32[416,128]{1,0:T(8,128)S(1)}) custom-call(s32[4]{0:T(128)S(1)} %add_add_fusion.1.sc, bf16[448,256]{1,0:T(8,128)(2,1)S(1)} %copy-done.6, bf16[448,256]{1,0:T(8,128)(2,1)S(1)} %collective-permute-done.20.refs_1_, bf16[448,256]{1,0:T(8,128)(2,1)S(1)} %collective-permute-done.21.refs_2_, ...), custom_call_target="tpu_custom_call" | custom-call | flops 137625600 | bytes 2920464 | tf_op jit(solution)/shard_map/pallas_call | solution.py:34
  127.7 3.2 %collective-permute-done.27 = bf16[8,3,32,512]{3,2,1,0:T(8,128)(2,1)} collective-permute-done((bf16[8,3,32,512]{3,2,1,0:T(8,128)(2,1)}, bf16[8,3,32,512]{3,2,1,0:T(8,128)(2,1)}, u32[]{:S(2)}, u32[]{:S(2)}) %collective-permute-start.27) | collective-permute-done | bytes 786464 | tf_op jit(solution)/shard_map/ppermute | solution.py:306
  130.9 2.8 %collective-permute-done.28 = bf16[8,3,32,512]{3,2,1,0:T(8,128)(2,1)} collective-permute-done((bf16[8,3,32,512]{3,2,1,0:T(8,128)(2,1)}, bf16[8,3,32,512]{3,2,1,0:T(8,128)(2,1)}, u32[]{:S(2)}, u32[]{:S(2)}) %collective-permute-start.28) | collective-permute-done | bytes 786464 | tf_op jit(solution)/shard_map/ppermute | solution.py:306
  137.4 2.5 %collective-permute-start.25 = (bf16[400,256]{1,0:T(8,128)(2,1)S(1)}, bf16[400,256]{1,0:T(8,128)(2,1)S(1)}, u32[]{:S(2)}, u32[]{:S(2)}) collective-permute-start(bf16[400,256]{1,0:T(8,128)(2,1)S(1)} %get-tuple-element.60.refs_0_), channel_id=1, source_target_pairs={{0,6},{2,0},{4,2},{6,4},{1,7},{3,1},{5,3},{7,5},{8,14},{10,8},{12,... | collective-permute-start | bytes 614408 | tf_op jit(solution)/shard_map/ppermute | solution.py:306
  139.9 8.9 %collective-permute-done.23.refs_1_ = bf16[400,256]{1,0:T(8,128)(2,1)S(1)} collective-permute-done((bf16[400,256]{1,0:T(8,128)(2,1)S(1)}, bf16[400,256]{1,0:T(8,128)(2,1)S(1)}, u32[]{:S(2)}, u32[]{:S(2)}) %collective-permute-start.23) | collective-permute-done | bytes 204832 | tf_op jit(solution)/shard_map/ppermute | solution.py:306
  149.5 4.0 %shard_map.77 = (bf16[432,256]{1,0:T(8,128)(2,1)S(1)}, bf16[432,256]{1,0:T(8,128)(2,1)S(1)}, bf16[432,256]{1,0:T(8,128)(2,1)S(1)}, bf16[432,256]{1,0:T(8,128)(2,...) custom-call(s32[4]{0:T(128)S(1)} %add_add_fusion.1.sc, bf16[400,256]{1,0:T(8,128)(2,1)S(1)} %get-tuple-element.60.refs_0_, ...), custom_call_target="tpu_custom_call" | custom-call | flops 1677721600 | bytes 11575312 | tf_op jit(solution)/shard_map/pallas_call | solution.py:34
  154.4 3.3 %collective-permute-start.31 = (bf16[432,256]{1,0:T(8,128)(2,1)S(1)}, bf16[432,256]{1,0:T(8,128)(2,1)S(1)}, u32[]{:S(2)}, u32[]{:S(2)}) collective-permute-start(bf16[432,256]{1,0:T(8,128)(2,1)S(1)} %get-tuple-element.70), channel_id=1, source_target_pairs={{0,4},{2,6},{4,0},{6,2},{1,5},{3,7},{5,1},{7,3},{8,12},{10,14},{12... | collective-permute-start | bytes 663560 | tf_op jit(solution)/shard_map/ppermute | solution.py:306
  157.6 4.1 %collective-permute-done.30.refs_1_ = bf16[432,256]{1,0:T(8,128)(2,1)S(1)} collective-permute-done((bf16[432,256]{1,0:T(8,128)(2,1)S(1)}, bf16[432,256]{1,0:T(8,128)(2,1)S(1)}, u32[]{:S(2)}, u32[]{:S(2)}) %collective-permute-start.30) | collective-permute-done | bytes 221216 | tf_op jit(solution)/shard_map/ppermute | solution.py:306
  161.8 5.9 %collective-permute-done.31.refs_2_ = bf16[432,256]{1,0:T(8,128)(2,1)S(1)} collective-permute-done((bf16[432,256]{1,0:T(8,128)(2,1)S(1)}, bf16[432,256]{1,0:T(8,128)(2,1)S(1)}, u32[]{:S(2)}, u32[]{:S(2)}) %collective-permute-start.31) | collective-permute-done | bytes 221216 | tf_op jit(solution)/shard_map/ppermute | solution.py:306
  170.2 3.3 %collective-permute-start.34 = (bf16[384,256]{1,0:T(8,128)(2,1)S(1)}, bf16[384,256]{1,0:T(8,128)(2,1)S(1)}, u32[]{:S(2)}, u32[]{:S(2)}) collective-permute-start(bf16[384,256]{1,0:T(8,128)(2,1)S(1)} %get-tuple-element.72.refs_0_), channel_id=1, source_target_pairs={{0,4},{2,6},{4,0},{6,2},{1,5},{3,7},{5,1},{7,3},{8,12},{10,14},{12... | collective-permute-start | bytes 589832 | tf_op jit(solution)/shard_map/ppermute | solution.py:306
  173.5 3.6 %collective-permute-done.33.refs_1_ = bf16[384,256]{1,0:T(8,128)(2,1)S(1)} collective-permute-done((bf16[384,256]{1,0:T(8,128)(2,1)S(1)}, bf16[384,256]{1,0:T(8,128)(2,1)S(1)}, u32[]{:S(2)}, u32[]{:S(2)}) %collective-permute-start.33) | collective-permute-done | bytes 196640 | tf_op jit(solution)/shard_map/ppermute | solution.py:306
  177.1 5.4 %collective-permute-done.34.refs_2_ = bf16[384,256]{1,0:T(8,128)(2,1)S(1)} collective-permute-done((bf16[384,256]{1,0:T(8,128)(2,1)S(1)}, bf16[384,256]{1,0:T(8,128)(2,1)S(1)}, u32[]{:S(2)}, u32[]{:S(2)}) %collective-permute-start.34) | collective-permute-done | bytes 196640 | tf_op jit(solution)/shard_map/ppermute | solution.py:306
  184.8 3.3 %collective-permute-start.37 = (f32[8,384]{1,0:T(8,128)S(1)}, f32[8,384]{1,0:T(8,128)S(1)}, u32[]{:S(2)}, u32[]{:S(2)}) collective-permute-start(f32[8,384]{1,0:T(8,128)S(1)} %get-tuple-element.76.refs_0_), channel_id=1, source_target_pairs={{0,4},{2,6},{4,0},{6,2},{1,5},{3,7},{5,1},{7,3},{8,12},{10,14},{12... | collective-permute-start | bytes 36872 | tf_op jit(solution)/shard_map/ppermute | solution.py:306
  (125 shorter events, 45.7 us)
Async XLA Ops:
  1.6 18.8 %all-to-all-start = ((bf16[8,1,32,512]{3,2,1,0:T(8,128)(2,1)}), bf16[8,1,32,512]{3,2,1,0:T(8,128)(2,1)S(1)}, u32[]{:S(2)}, u32[]{:S(2)}) async-start(bf16[8,1,32,512]{3,2,1,0:T(8,128)(2,1)} %broadcast_in_dim.9), calls=%async_computation | async-start | bytes 524288 | tf_op jit(solution)/shard_map/all_to_all | solution.py:319
  9.5 19.0 %collective-permute-start = (bf16[24,512]{1,0:T(8,128)(2,1)S(1)}, bf16[24,512]{1,0:T(8,128)(2,1)S(1)}, u32[]{:S(2)}, u32[]{:S(2)}) collective-permute-start(bf16[24,512]{1,0:T(8,128)(2,1)S(1)} %get-tuple-element.84), channel_id=1, source_target_pairs={{0,8},{8,16},{16,24},{24,32},{32,40},{40,48},{48,56},{56,64},{64,7... | collective-permute-start | bytes 73736 | tf_op jit(solution)/shard_map/ppermute | solution.py:365
  13.0 19.0 %collective-permute-start.1 = (bf16[24,512]{1,0:T(8,128)(2,1)S(1)}, bf16[24,512]{1,0:T(8,128)(2,1)S(1)}, u32[]{:S(2)}, u32[]{:S(2)}) collective-permute-start(bf16[24,512]{1,0:T(8,128)(2,1)S(1)} %get-tuple-element.83), channel_id=1, source_target_pairs={{8,0},{16,8},{24,16},{32,24},{40,32},{48,40},{56,48},{64,56},{72,6... | collective-permute-start | bytes 73736 | tf_op jit(solution)/shard_map/ppermute | solution.py:366
  21.2 32.7 %all-to-all-start.1 = ((bf16[8,2,32,512]{3,2,1,0:T(8,128)(2,1)}), bf16[8,2,32,512]{3,2,1,0:T(8,128)(2,1)}, u32[]{:S(2)}, u32[]{:S(2)}) async-start(bf16[8,2,32,512]{3,2,1,0:T(8,128)(2,1)} %broadcast_in_dim.10), calls=%async_computation.1 | async-start | bytes 1048576 | tf_op jit(solution)/shard_map/all_to_all | solution.py:319
  28.6 13.2 %collective-permute-start.4 = (bf16[8,1,32,512]{3,2,0,1:T(8,128)(2,1)S(1)}, bf16[8,1,32,512]{3,2,0,1:T(8,128)(2,1)S(1)}, u32[]{:S(2)}, u32[]{:S(2)}) collective-permute-start(bf16[8,1,32,512]{3,2,0,1:T(8,128)(2,1)S(1)} %bitcast.24), channel_id=1, source_target_pairs={{0,8},{8,16},{16,24},{24,0},{1,9},{9,17},{17,25},{25,1},{2,10},{10... | collective-permute-start | bytes 786440 | tf_op jit(solution)/shard_map/ppermute | solution.py:306
  28.6 13.3 %collective-permute-start.5 = (bf16[8,1,32,512]{3,2,0,1:T(8,128)(2,1)S(1)}, bf16[8,1,32,512]{3,2,0,1:T(8,128)(2,1)S(1)}, u32[]{:S(2)}, u32[]{:S(2)}) collective-permute-start(bf16[8,1,32,512]{3,2,0,1:T(8,128)(2,1)S(1)} %bitcast.25), channel_id=1, source_target_pairs={{0,16},{8,24},{16,0},{24,8},{1,17},{9,25},{17,1},{25,9},{2,18},{10... | collective-permute-start | bytes 786440 | tf_op jit(solution)/shard_map/ppermute | solution.py:306
  30.4 12.0 %collective-permute-start.6 = (bf16[8,1,32,512]{3,2,0,1:T(8,128)(2,1)S(1)}, bf16[8,1,32,512]{3,2,0,1:T(8,128)(2,1)S(1)}, u32[]{:S(2)}, u32[]{:S(2)}) collective-permute-start(bf16[8,1,32,512]{3,2,0,1:T(8,128)(2,1)S(1)} %bitcast.26), channel_id=1, source_target_pairs={{0,24},{8,0},{16,8},{24,16},{1,25},{9,1},{17,9},{25,17},{2,26},{10... | collective-permute-start | bytes 786440 | tf_op jit(solution)/shard_map/ppermute | solution.py:306
  50.9 9.4 %collective-permute-start.10 = (bf16[432,256]{1,0:T(8,128)(2,1)}, bf16[432,256]{1,0:T(8,128)(2,1)S(1)}, u32[]{:S(2)}, u32[]{:S(2)}) collective-permute-start(bf16[432,256]{1,0:T(8,128)(2,1)} %get-tuple-element.48), channel_id=1, source_target_pairs={{0,4},{2,6},{4,0},{6,2},{1,5},{3,7},{5,1},{7,3},{8,12},{10,14},{12... | collective-permute-start | bytes 663560 | tf_op jit(solution)/shard_map/ppermute | solution.py:306
  53.9 18.6 %collective-permute-start.15 = (bf16[8,2,32,512]{3,2,1,0:T(8,128)(2,1)}, bf16[8,2,32,512]{3,2,1,0:T(8,128)(2,1)}, u32[]{:S(2)}, u32[]{:S(2)}) collective-permute-start(bf16[8,2,32,512]{3,2,1,0:T(8,128)(2,1)} %all-to-all-done.1), channel_id=1, source_target_pairs={{0,8},{8,16},{16,24},{24,0},{1,9},{9,17},{17,25},{25,1},{2,10},{10... | collective-permute-start | bytes 1572872 | tf_op jit(solution)/shard_map/ppermute | solution.py:306
  54.2 27.1 %collective-permute-start.16 = (bf16[8,2,32,512]{3,2,1,0:T(8,128)(2,1)}, bf16[8,2,32,512]{3,2,1,0:T(8,128)(2,1)}, u32[]{:S(2)}, u32[]{:S(2)}) collective-permute-start(bf16[8,2,32,512]{3,2,1,0:T(8,128)(2,1)} %all-to-all-done.1), channel_id=1, source_target_pairs={{0,16},{8,24},{16,0},{24,8},{1,17},{9,25},{17,1},{25,9},{2,18},{10... | collective-permute-start | bytes 1572872 | tf_op jit(solution)/shard_map/ppermute | solution.py:306
  57.8 23.5 %collective-permute-start.17 = (bf16[8,2,32,512]{3,2,1,0:T(8,128)(2,1)}, bf16[8,2,32,512]{3,2,1,0:T(8,128)(2,1)}, u32[]{:S(2)}, u32[]{:S(2)}) collective-permute-start(bf16[8,2,32,512]{3,2,1,0:T(8,128)(2,1)} %all-to-all-done.1), channel_id=1, source_target_pairs={{0,24},{8,0},{16,8},{24,16},{1,25},{9,1},{17,9},{25,17},{2,26},{10... | collective-permute-start | bytes 1572872 | tf_op jit(solution)/shard_map/ppermute | solution.py:306
  57.8 12.9 %collective-permute-start.11 = (bf16[432,256]{1,0:T(8,128)(2,1)}, bf16[432,256]{1,0:T(8,128)(2,1)S(1)}, u32[]{:S(2)}, u32[]{:S(2)}) collective-permute-start(bf16[432,256]{1,0:T(8,128)(2,1)} %copy-done.13), channel_id=1, source_target_pairs={{0,6},{2,0},{4,2},{6,4},{1,7},{3,1},{5,3},{7,5},{8,14},{10,8},{12,... | collective-permute-start | bytes 663560 | tf_op jit(solution)/shard_map/ppermute | solution.py:306
  60.3 10.4 %collective-permute-start.9 = (bf16[432,256]{1,0:T(8,128)(2,1)}, bf16[432,256]{1,0:T(8,128)(2,1)S(1)}, u32[]{:S(2)}, u32[]{:S(2)}) collective-permute-start(bf16[432,256]{1,0:T(8,128)(2,1)} %copy-done.12), channel_id=1, source_target_pairs={{0,2},{2,4},{4,6},{6,0},{1,3},{3,5},{5,7},{7,1},{8,10},{10,12},{12... | collective-permute-start | bytes 663560 | tf_op jit(solution)/shard_map/ppermute | solution.py:306
  63.4 24.0 %all-to-all-start.2 = ((bf16[8,3,32,512]{3,2,1,0:T(8,128)(2,1)}), bf16[8,3,32,512]{3,2,1,0:T(8,128)(2,1)}, u32[]{:S(2)}, u32[]{:S(2)}) async-start(bf16[8,3,32,512]{3,2,1,0:T(8,128)(2,1)} %broadcast_in_dim.11), calls=%async_computation.2 | async-start | bytes 1572864 | tf_op jit(solution)/shard_map/all_to_all | solution.py:319
  83.6 17.5 %collective-permute-start.19 = (bf16[2,8,2,32,512]{4,3,2,1,0:T(8,128)(2,1)}, bf16[2,8,2,32,512]{4,3,2,1,0:T(8,128)(2,1)}, u32[]{:S(2)}, u32[]{:S(2)}) collective-permute-start(bf16[2,8,2,32,512]{4,3,2,1,0:T(8,128)(2,1)} %pad_maximum_fusion.2.refs_9_), channel_id=1, source_target_pairs={{0,1},{1,0},{2,3},{3,2},{4,5},{5,4},{6,7},{7,6},{8,9},{9,8},{10,11... | collective-permute-start | bytes 3145736 | tf_op jit(solution)/shard_map/ppermute | solution.py:310
  83.6 17.6 %collective-permute-start.18 = (bf16[2,8,2,32,512]{4,3,2,1,0:T(8,128)(2,1)}, bf16[2,8,2,32,512]{4,3,2,1,0:T(8,128)(2,1)}, u32[]{:S(2)}, u32[]{:S(2)}) collective-permute-start(bf16[2,8,2,32,512]{4,3,2,1,0:T(8,128)(2,1)} %pad_maximum_fusion.1.refs_8_), channel_id=1, source_target_pairs={{0,1},{1,0},{2,3},{3,2},{4,5},{5,4},{6,7},{7,6},{8,9},{9,8},{10,11... | collective-permute-start | bytes 3145736 | tf_op jit(solution)/shard_map/ppermute | solution.py:310
  84.1 12.9 %collective-permute-start.12 = (bf16[416,256]{1,0:T(8,128)(2,1)S(1)}, bf16[416,256]{1,0:T(8,128)(2,1)S(1)}, u32[]{:S(2)}, u32[]{:S(2)}) collective-permute-start(bf16[416,256]{1,0:T(8,128)(2,1)S(1)} %shard_map.74.refs_0_), channel_id=1, source_target_pairs={{0,2},{2,4},{4,6},{6,0},{1,3},{3,5},{5,7},{7,1},{8,10},{10,12},{12... | collective-permute-start | bytes 638984 | tf_op jit(solution)/shard_map/ppermute | solution.py:306
  84.7 12.6 %collective-permute-start.13 = (bf16[416,256]{1,0:T(8,128)(2,1)S(1)}, bf16[416,256]{1,0:T(8,128)(2,1)S(1)}, u32[]{:S(2)}, u32[]{:S(2)}) collective-permute-start(bf16[416,256]{1,0:T(8,128)(2,1)S(1)} %shard_map.74.refs_0_), channel_id=1, source_target_pairs={{0,4},{2,6},{4,0},{6,2},{1,5},{3,7},{5,1},{7,3},{8,12},{10,14},{12... | collective-permute-start | bytes 638984 | tf_op jit(solution)/shard_map/ppermute | solution.py:306
  86.7 14.4 %collective-permute-start.14 = (bf16[416,256]{1,0:T(8,128)(2,1)S(1)}, bf16[416,256]{1,0:T(8,128)(2,1)S(1)}, u32[]{:S(2)}, u32[]{:S(2)}) collective-permute-start(bf16[416,256]{1,0:T(8,128)(2,1)S(1)} %shard_map.74.refs_0_), channel_id=1, source_target_pairs={{0,6},{2,0},{4,2},{6,4},{1,7},{3,1},{5,3},{7,5},{8,14},{10,8},{12,... | collective-permute-start | bytes 638984 | tf_op jit(solution)/shard_map/ppermute | solution.py:306
  97.0 30.7 %collective-permute-start.26 = (bf16[8,3,32,512]{3,2,1,0:T(8,128)(2,1)}, bf16[8,3,32,512]{3,2,1,0:T(8,128)(2,1)S(1)}, u32[]{:S(2)}, u32[]{:S(2)}) collective-permute-start(bf16[8,3,32,512]{3,2,1,0:T(8,128)(2,1)} %all-to-all-done.2), channel_id=1, source_target_pairs={{0,8},{8,16},{16,24},{24,0},{1,9},{9,17},{17,25},{25,1},{2,10},{10... | collective-permute-start | bytes 2359304 | tf_op jit(solution)/shard_map/ppermute | solution.py:306
  97.3 33.6 %collective-permute-start.27 = (bf16[8,3,32,512]{3,2,1,0:T(8,128)(2,1)}, bf16[8,3,32,512]{3,2,1,0:T(8,128)(2,1)}, u32[]{:S(2)}, u32[]{:S(2)}) collective-permute-start(bf16[8,3,32,512]{3,2,1,0:T(8,128)(2,1)} %all-to-all-done.2), channel_id=1, source_target_pairs={{0,16},{8,24},{16,0},{24,8},{1,17},{9,25},{17,1},{25,9},{2,18},{10... | collective-permute-start | bytes 2359304 | tf_op jit(solution)/shard_map/ppermute | solution.py:306
  101.1 32.6 %collective-permute-start.28 = (bf16[8,3,32,512]{3,2,1,0:T(8,128)(2,1)}, bf16[8,3,32,512]{3,2,1,0:T(8,128)(2,1)}, u32[]{:S(2)}, u32[]{:S(2)}) collective-permute-start(bf16[8,3,32,512]{3,2,1,0:T(8,128)(2,1)} %all-to-all-done.2), channel_id=1, source_target_pairs={{0,24},{8,0},{16,8},{24,16},{1,25},{9,1},{17,9},{25,17},{2,26},{10... | collective-permute-start | bytes 2359304 | tf_op jit(solution)/shard_map/ppermute | solution.py:306
  109.5 8.9 %collective-permute-start.20 = (bf16[448,256]{1,0:T(8,128)(2,1)}, bf16[448,256]{1,0:T(8,128)(2,1)S(1)}, u32[]{:S(2)}, u32[]{:S(2)}) collective-permute-start(bf16[448,256]{1,0:T(8,128)(2,1)} %get-tuple-element.57), channel_id=1, source_target_pairs={{0,2},{2,4},{4,6},{6,0},{1,3},{3,5},{5,7},{7,1},{8,10},{10,12},{12... | collective-permute-start | bytes 688136 | tf_op jit(solution)/shard_map/ppermute | solution.py:306
  109.5 12.4 %collective-permute-start.21 = (bf16[448,256]{1,0:T(8,128)(2,1)}, bf16[448,256]{1,0:T(8,128)(2,1)S(1)}, u32[]{:S(2)}, u32[]{:S(2)}) collective-permute-start(bf16[448,256]{1,0:T(8,128)(2,1)} %get-tuple-element.58), channel_id=1, source_target_pairs={{0,4},{2,6},{4,0},{6,2},{1,5},{3,7},{5,1},{7,3},{8,12},{10,14},{12... | collective-permute-start | bytes 688136 | tf_op jit(solution)/shard_map/ppermute | solution.py:306
  135.6 13.8 %collective-permute-start.29 = (bf16[4,8,3,32,512]{4,3,2,1,0:T(8,128)(2,1)S(1)}, bf16[4,8,3,32,512]{4,3,2,1,0:T(8,128)(2,1)S(1)}, u32[]{:S(2)}, u32[]{:S(2)}) collective-permute-start(bf16[4,8,3,32,512]{4,3,2,1,0:T(8,128)(2,1)S(1)} %pad_maximum_fusion.refs_9_), channel_id=1, source_target_pairs={{0,1},{1,0},{2,3},{3,2},{4,5},{5,4},{6,7},{7,6},{8,9},{9,8},{10,11... | collective-permute-start | bytes 9437192 | tf_op jit(solution)/shard_map/ppermute | solution.py:310
  135.7 13.1 %collective-permute-start.23 = (bf16[400,256]{1,0:T(8,128)(2,1)S(1)}, bf16[400,256]{1,0:T(8,128)(2,1)S(1)}, u32[]{:S(2)}, u32[]{:S(2)}) collective-permute-start(bf16[400,256]{1,0:T(8,128)(2,1)S(1)} %get-tuple-element.60.refs_0_), channel_id=1, source_target_pairs={{0,2},{2,4},{4,6},{6,0},{1,3},{3,5},{5,7},{7,1},{8,10},{10,12},{12... | collective-permute-start | bytes 614408 | tf_op jit(solution)/shard_map/ppermute | solution.py:306
  135.8 13.0 %collective-permute-start.24 = (bf16[400,256]{1,0:T(8,128)(2,1)S(1)}, bf16[400,256]{1,0:T(8,128)(2,1)S(1)}, u32[]{:S(2)}, u32[]{:S(2)}) collective-permute-start(bf16[400,256]{1,0:T(8,128)(2,1)S(1)} %get-tuple-element.60.refs_0_), channel_id=1, source_target_pairs={{0,4},{2,6},{4,0},{6,2},{1,5},{3,7},{5,1},{7,3},{8,12},{10,14},{12... | collective-permute-start | bytes 614408 | tf_op jit(solution)/shard_map/ppermute | solution.py:306
  137.4 12.0 %collective-permute-start.25 = (bf16[400,256]{1,0:T(8,128)(2,1)S(1)}, bf16[400,256]{1,0:T(8,128)(2,1)S(1)}, u32[]{:S(2)}, u32[]{:S(2)}) collective-permute-start(bf16[400,256]{1,0:T(8,128)(2,1)S(1)} %get-tuple-element.60.refs_0_), channel_id=1, source_target_pairs={{0,6},{2,0},{4,2},{6,4},{1,7},{3,1},{5,3},{7,5},{8,14},{10,8},{12,... | collective-permute-start | bytes 614408 | tf_op jit(solution)/shard_map/ppermute | solution.py:306
  154.4 13.3 %collective-permute-start.31 = (bf16[432,256]{1,0:T(8,128)(2,1)S(1)}, bf16[432,256]{1,0:T(8,128)(2,1)S(1)}, u32[]{:S(2)}, u32[]{:S(2)}) collective-permute-start(bf16[432,256]{1,0:T(8,128)(2,1)S(1)} %get-tuple-element.70), channel_id=1, source_target_pairs={{0,4},{2,6},{4,0},{6,2},{1,5},{3,7},{5,1},{7,3},{8,12},{10,14},{12... | collective-permute-start | bytes 663560 | tf_op jit(solution)/shard_map/ppermute | solution.py:306
  157.6 10.1 %collective-permute-start.32 = (bf16[432,256]{1,0:T(8,128)(2,1)S(1)}, bf16[432,256]{1,0:T(8,128)(2,1)S(1)}, u32[]{:S(2)}, u32[]{:S(2)}) collective-permute-start(bf16[432,256]{1,0:T(8,128)(2,1)S(1)} %get-tuple-element.71), channel_id=1, source_target_pairs={{0,6},{2,0},{4,2},{6,4},{1,7},{3,1},{5,3},{7,5},{8,14},{10,8},{12,... | collective-permute-start | bytes 663560 | tf_op jit(solution)/shard_map/ppermute | solution.py:306
  170.2 12.3 %collective-permute-start.34 = (bf16[384,256]{1,0:T(8,128)(2,1)S(1)}, bf16[384,256]{1,0:T(8,128)(2,1)S(1)}, u32[]{:S(2)}, u32[]{:S(2)}) collective-permute-start(bf16[384,256]{1,0:T(8,128)(2,1)S(1)} %get-tuple-element.72.refs_0_), channel_id=1, source_target_pairs={{0,4},{2,6},{4,0},{6,2},{1,5},{3,7},{5,1},{7,3},{8,12},{10,14},{12... | collective-permute-start | bytes 589832 | tf_op jit(solution)/shard_map/ppermute | solution.py:306
  173.5 9.0 %collective-permute-start.35 = (bf16[384,256]{1,0:T(8,128)(2,1)S(1)}, bf16[384,256]{1,0:T(8,128)(2,1)S(1)}, u32[]{:S(2)}, u32[]{:S(2)}) collective-permute-start(bf16[384,256]{1,0:T(8,128)(2,1)S(1)} %get-tuple-element.72.refs_0_), channel_id=1, source_target_pairs={{0,6},{2,0},{4,2},{6,4},{1,7},{3,1},{5,3},{7,5},{8,14},{10,8},{12,... | collective-permute-start | bytes 589832 | tf_op jit(solution)/shard_map/ppermute | solution.py:306
  (31 other events, 380.2 us)
